TPU v7x, 256 devices: a whole 4x4x8 slice. The times are simulated.
256 devices in a mesh: sp: 32 (over z, y), tp: 8 (over x, core).
Axes of the slice: x: 4, y: 4, z: 8, core: 2. Of those that a mesh axis runs over, the one named last changes fastest.
Arguments:
- mix_input: bfloat16 [8192, 1024], P('sp', 'tp'), may hold values from -6 to 6
- stream: bfloat16 [8192, 2048], P(('sp', 'tp')), may hold values from -48 to 48
- doc_ids: int32 [8192], P('sp'), may hold values from 0 to 3, never falling along the last dimension, each value on 1 to 4096 neighbouring positions
- log_dt: float32 [64], P('tp'), may hold values from -12 to -2
- decay_rate: float32 [64, 64], P('tp'), may hold values from 0.5 to 1
- frequency: float32 [64, 64], P('tp'), may hold values from 0 to 64
- input_real: float32 [2, 64, 64, 16], P(None, 'tp'), may hold values from -400 to 400
- input_imag: float32 [2, 64, 64, 16], P(None, 'tp'), may hold values from -400 to 400
- output_real: float32 [2, 64, 16, 64], P(None, 'tp'), may hold values from -0.75 to 0.75
- output_imag: float32 [2, 64, 16, 64], P(None, 'tp'), may hold values from -0.75 to 0.75
- skip_gain: float32 [1024], P('tp'), may hold values from -4 to 4
- log_keep: float32 [64, 8192], P('tp', 'sp'), may hold values from -2 to 0
- proj_weight: bfloat16 [1024, 2048], P('tp'), may hold values from -0.1875 to 0.1875
- norm_gain: float32 [2048], replicated, may hold values from 0.1 to 1.9
- gate_weight: bfloat16 [2048, 5632], P('sp', 'tp'), may hold values from -0.125 to 0.125
- up_weight: bfloat16 [2048, 5632], P('sp', 'tp'), may hold values from -0.125 to 0.125
- down_weight: bfloat16 [5632, 2048], P('tp', 'sp'), may hold values from -0.078125 to 0.078125
Outputs:
- layer_out: bfloat16 [8192, 2048], P(('sp', 'tp'))
Inputs may be any that keep to these rules, and one draw needn't show every extreme that they name: `doc_ids`: document numbers never fall along the positions; a document covers at most half of the positions.
All inputs are finite; a program needn't handle non-finite values.
Results may differ from a plain program's by a relative error of at most 0.009.
Values may be sent and summed in bfloat16 or wider, within the bound.
A program may use at most 128 MiB of HBM per device.

v0:
```python
import jax
import jax.numpy as jnp
from jax import lax
from jax.sharding import Mesh
from jax.sharding import PartitionSpec as P

GROUP = 16
SP = ("sp_0", "sp_1")
SP_TP = ("sp_0", "sp_1", "tp")


HIGHEST = lax.Precision.HIGHEST


def from_everyone(array, axis):
    copies = jnp.broadcast_to(array, (lax.axis_size(axis), *array.shape))
    return lax.all_to_all(copies, axis, split_axis=0, concat_axis=0, tiled=True)


def all_in_one(array, axis):
    leaves = jax.tree.leaves(array)
    turns = sorted(range(len(leaves)), key=lambda k: -leaves[k].size)
    width = (1, *leaves[turns[0]].shape)[-1]
    lines = [
        jnp.pad(leaves[k].reshape(-1), (0, -leaves[k].size % width)).reshape(-1, width)
        for k in turns
    ]
    both, at, found = (from_everyone(jnp.concatenate(lines), axis), 0, {})
    for k, line in zip(turns, lines):
        section = both[:, at : at + len(line)].reshape(len(both), -1)
        found[k] = section[:, : leaves[k].size].reshape(-1, *leaves[k].shape)
        at += len(line)
    numbers = iter(range(len(leaves)))
    return jax.tree.map(lambda _: found[next(numbers)], array)


def folded_in_pairs(pieces, combine):
    while len(jax.tree.leaves(pieces)[0]) > 1:
        pieces = jax.vmap(combine)(
            *(jax.tree.map(lambda part: part[side::2], pieces) for side in (0, 1))
        )
    return jax.tree.map(lambda part: part[0], pieces)


def carried_in(array, axis, combine, identity, reverse):
    devices, here = (lax.axis_size(axis), lax.axis_index(axis))
    passed = jnp.arange(devices) > here if reverse else jnp.arange(devices) < here

    def kept(part, zero, own):
        part = jnp.where(
            passed.reshape(-1, *(1 for _ in own.shape)), part, jnp.asarray(zero, own.dtype)
        )
        return part[::-1] if reverse else part

    pieces = all_in_one(array, axis)
    return folded_in_pairs(jax.tree.map(kept, pieces, identity, array), combine)


def whole_of(array, axes, dim):
    for axis in reversed(axes):
        array = lax.all_gather(array, axis, axis=dim, tiled=True)
    return array


def split_up(array, dim, devices):
    before, after = (array.shape[:dim], array.shape[dim + 1 :])
    return jnp.moveaxis(array.reshape(*before, devices, -1, *after), dim, 0)


def summed_on_arrival(array, axis, dim):
    blocks = split_up(array, dim, lax.axis_size(axis))
    arrived = lax.all_to_all(blocks, axis, split_axis=0, concat_axis=0, tiled=True)
    return arrived.astype(jnp.float32).sum(axis=0)


def laid_out(blocks, dim):
    blocks = jnp.moveaxis(blocks, 0, dim)
    shape = blocks.shape
    return blocks.reshape(*shape[:dim], shape[dim] * shape[dim + 1], *shape[dim + 2 :])


def gather_directly(array, axis, dim):
    return laid_out(from_everyone(array, axis), dim)


def discretize(log_dt, decay_rate, frequency):
    step_size = jnp.exp(log_dt)[:, None]
    magnitude = jnp.exp(-step_size * decay_rate)
    angle_step = step_size * frequency
    state_real = magnitude * jnp.cos(angle_step)
    state_imag = magnitude * jnp.sin(angle_step)
    denominator = decay_rate * decay_rate + frequency * frequency
    shifted = state_real - 1.0
    zoh_real = (-shifted * decay_rate + state_imag * frequency) / denominator
    holdfixed_angle_part = (-state_imag * decay_rate - shifted * frequency) / denominator
    return (state_real, state_imag, zoh_real, holdfixed_angle_part)


def input_maps(zoh_real, holdfixed_angle_part, input_real, input_imag):
    scale_real = zoh_real[None, :, :, None]
    scale_imag = holdfixed_angle_part[None, :, :, None]
    return (
        scale_real * input_real - scale_imag * input_imag,
        scale_real * input_imag + scale_imag * input_real,
    )


def pair_combine(earlier, later):
    mult_one_real, mult_one_imag, first_state_real, state_one_imag = earlier
    mult_two_real, second_multiplier_imag, state_two_real, state_two_imag = later
    return (
        mult_two_real * mult_one_real - second_multiplier_imag * mult_one_imag,
        mult_two_real * mult_one_imag + second_multiplier_imag * mult_one_real,
        mult_two_real * first_state_real - second_multiplier_imag * state_one_imag + state_two_real,
        mult_two_real * state_one_imag + second_multiplier_imag * first_state_real + state_two_imag,
    )


def blocked_scan(mult_real, mult_imag, drive_real, drive_imag, reverse):
    tokens_here, width = mult_real.shape
    span = min(16, tokens_here)
    count = tokens_here // span
    block_mr, block_mi, block_dr, block_di = (
        item.reshape(count, span, width) for item in (mult_real, mult_imag, drive_real, drive_imag)
    )
    running_pr = jnp.ones((count, width), jnp.float32)
    running_pi = jnp.zeros((count, width), jnp.float32)
    running_sr = jnp.zeros((count, width), jnp.float32)
    running_si = jnp.zeros((count, width), jnp.float32)
    slots = [None] * span
    positions = range(span - 1, -1, -1) if reverse else range(span)
    for place in positions:
        step_real = block_mr[:, place]
        step_imag = block_mi[:, place]
        running_pr, running_pi = (
            step_real * running_pr - step_imag * running_pi,
            step_real * running_pi + step_imag * running_pr,
        )
        running_sr, running_si = (
            step_real * running_sr - step_imag * running_si + block_dr[:, place],
            step_real * running_si + step_imag * running_sr + block_di[:, place],
        )
        slots[place] = (running_pr, running_pi, running_sr, running_si)
    inner = tuple((jnp.stack([slot[member] for slot in slots], axis=1) for member in range(4)))
    edge = 0 if reverse else span - 1
    ends = tuple((item[:, edge] for item in inner))
    outer = lax.associative_scan(pair_combine, ends, reverse=reverse, axis=0)
    ones_row = jnp.ones((1, width), jnp.float32)
    zero_row = jnp.zeros((1, width), jnp.float32)
    neutral = (ones_row, zero_row, zero_row, zero_row)
    if reverse:
        carry = tuple(
            (jnp.concatenate([item[1:], blank], axis=0) for item, blank in zip(outer, neutral))
        )
    else:
        carry = tuple(
            (jnp.concatenate([blank, item[:-1]], axis=0) for item, blank in zip(outer, neutral))
        )
    carry_mr, carry_mi, carry_sr, carry_si = (item[:, None, :] for item in carry)
    inner_mr, inner_mi, inner_sr, inner_si = inner
    prod_real = inner_mr * carry_mr - inner_mi * carry_mi
    prod_imag = inner_mr * carry_mi + inner_mi * carry_mr
    local_real = inner_sr + inner_mr * carry_sr - inner_mi * carry_si
    local_imag = inner_si + inner_mr * carry_si + inner_mi * carry_sr
    return tuple(
        (
            item.reshape(tokens_here, width)
            for item in (prod_real, prod_imag, local_real, local_imag)
        )
    )


def chain_combine(earlier, later):
    early_real, early_imag, early_state_real, early_state_imag, early_near, early_far = earlier
    late_real, late_imag, late_state_real, late_state_imag, late_near, late_far = later
    joined = (late_near == early_far) | (early_far < 0.0) | (late_near < 0.0)
    linked = jnp.where(joined, 1.0, 0.0).astype(jnp.float32)
    step_real = linked * late_real
    step_imag = linked * late_imag
    return (
        step_real * early_real - step_imag * early_imag,
        step_real * early_imag + step_imag * early_real,
        step_real * early_state_real - step_imag * early_state_imag + late_state_real,
        step_real * early_state_imag + step_imag * early_state_real + late_state_imag,
        jnp.where(early_near < 0.0, late_near, early_near),
        jnp.where(late_far < 0.0, early_far, late_far),
    )


def direction_pass(
    grouped,
    doc_ids,
    keep_rates,
    state_real,
    state_imag,
    map_real,
    map_imag,
    read_real,
    read_imag,
    reverse,
):
    tokens_here, groups_here, group_width = grouped.shape
    states_here = state_real.shape[1]
    flat_width = groups_here * states_here
    drive_real = jnp.einsum("tgi,gpi->tgp", grouped, map_real, precision=HIGHEST).reshape(
        tokens_here, flat_width
    )
    drive_imag = jnp.einsum("tgi,gpi->tgp", grouped, map_imag, precision=HIGHEST).reshape(
        tokens_here, flat_width
    )
    same_doc = (doc_ids[1:] == doc_ids[:-1]).astype(jnp.float32)
    single = jnp.ones((1,), jnp.float32)
    doc_links = (
        jnp.concatenate([same_doc, single]) if reverse else jnp.concatenate([single, same_doc])
    )
    factor = keep_rates[:, :, None] * doc_links[:, None, None]
    mult_real = (factor * state_real[None]).reshape(tokens_here, flat_width)
    mult_imag = (factor * state_imag[None]).reshape(tokens_here, flat_width)
    prod_real, prod_imag, local_real, local_imag = blocked_scan(
        mult_real, mult_imag, drive_real, drive_imag, reverse
    )
    far_end = 0 if reverse else tokens_here - 1
    near_end = tokens_here - 1 if reverse else 0
    doc_values = doc_ids.astype(jnp.float32)
    summary = (
        prod_real[far_end],
        prod_imag[far_end],
        local_real[far_end],
        local_imag[far_end],
        doc_values[near_end],
        doc_values[far_end],
    )
    neutral = (
        jnp.ones((flat_width,), jnp.float32),
        jnp.zeros((flat_width,), jnp.float32),
        jnp.zeros((flat_width,), jnp.float32),
        jnp.zeros((flat_width,), jnp.float32),
        jnp.array(-1.0, jnp.float32),
        jnp.array(-1.0, jnp.float32),
    )
    carried = carried_in(summary, SP, chain_combine, neutral, reverse)
    joined = (doc_values[near_end] == carried[5]).astype(jnp.float32)
    enter_real = joined * carried[2]
    enter_imag = joined * carried[3]
    full_real = local_real + prod_real * enter_real[None] - prod_imag * enter_imag[None]
    full_imag = local_imag + prod_real * enter_imag[None] + prod_imag * enter_real[None]
    result = jnp.einsum(
        "tgp,gip->tgi",
        full_real.reshape(tokens_here, groups_here, states_here),
        read_real,
        precision=HIGHEST,
    )
    result = result - jnp.einsum(
        "tgp,gip->tgi",
        full_imag.reshape(tokens_here, groups_here, states_here),
        read_imag,
        precision=HIGHEST,
    )
    return result.reshape(tokens_here, groups_here * group_width)


def local(
    mix_input,
    stream,
    doc_ids,
    log_dt,
    decay_rate,
    frequency,
    input_real,
    input_imag,
    output_real,
    output_imag,
    skip_gain,
    log_keep,
    proj_weight,
    norm_gain,
    gate_weight,
    up_weight,
    down_weight,
):
    gate_whole, up_whole = (whole_of(gate_weight, SP, 0), whole_of(up_weight, SP, 0))
    down_whole = whole_of(down_weight, SP, 1)
    state_real, state_imag, zoh_real, holdfixed_angle_part = discretize(
        log_dt, decay_rate, frequency
    )
    map_real, map_imag = input_maps(zoh_real, holdfixed_angle_part, input_real, input_imag)
    tokens_here = mix_input.shape[0]
    channels = mix_input.astype(jnp.float32)
    grouped = channels.reshape(tokens_here, log_dt.shape[0], GROUP)
    keep_rates = jnp.exp(log_keep).T
    mixed_pre = skip_gain * channels
    for direction, reverse in ((0, False), (1, True)):
        mixed_pre = mixed_pre + direction_pass(
            grouped,
            doc_ids,
            keep_rates,
            state_real,
            state_imag,
            map_real[direction],
            map_imag[direction],
            output_real[direction],
            output_imag[direction],
            reverse,
        )
    mixed = jax.nn.gelu(mixed_pre).astype(jnp.bfloat16)
    branch = summed_on_arrival(
        jnp.dot(mixed, proj_weight, preferred_element_type=jnp.float32).astype(jnp.bfloat16),
        "tp",
        0,
    )
    resid = stream.astype(jnp.float32) + branch
    scale = lax.rsqrt(jnp.mean(resid * resid, axis=-1, keepdims=True) + 1e-06)
    normed = (resid * scale * norm_gain).astype(jnp.bfloat16)
    rows_all = gather_directly(normed, "tp", 0)
    gate = jnp.dot(rows_all, gate_whole, preferred_element_type=jnp.float32)
    upward = jnp.dot(rows_all, up_whole, preferred_element_type=jnp.float32)
    hidden = (jax.nn.silu(gate) * upward).astype(jnp.bfloat16)
    partial_out = jnp.dot(hidden, down_whole, preferred_element_type=jnp.float32)
    ffn = summed_on_arrival(partial_out.astype(jnp.bfloat16), "tp", 0)
    return (resid + 0.5 * ffn).astype(jnp.bfloat16)


def solution(mesh):
    torus = Mesh(mesh.devices.reshape(8, 4, mesh.shape["tp"]), ("sp_0", "sp_1", "tp"))
    in_specs = (
        P(SP, "tp"),
        P(SP_TP, None),
        P(SP),
        P("tp"),
        P("tp", None),
        P("tp", None),
        P(None, "tp", None, None),
        P(None, "tp", None, None),
        P(None, "tp", None, None),
        P(None, "tp", None, None),
        P("tp"),
        P("tp", SP),
        P("tp", None),
        P(),
        P(SP, "tp"),
        P(SP, "tp"),
        P("tp", SP),
    )
    out_specs = P(SP_TP, None)
    return jax.shard_map(local, mesh=torus, in_specs=in_specs, out_specs=out_specs, check_vma=False)
```

profile of v0, /device:TPU:1, one launch (start us, length us, event | category | flops | bytes accessed | tf_op | source)
XLA Modules:
  0.0 346.8 jit_solution(15707418047209030419)
XLA Ops:
  6.5 13.1 %all_gather.18 = bf16[256,704]{1,0:T(8,128)(2,1)} all-gather(bf16[64,704]{1,0:T(8,128)(2,1)} %param.31), channel_id=1, replica_groups=mesh['sp_0'=8,'sp_1'=4,'tp'=8] {'sp_1'}, dimensions={0}, use_global_device_ids=true | all-gather | bytes 450560 | tf_op jit(solution)/shard_map/all_gather | solution.py:61
  19.8 10.7 %all_gather.20 = bf16[256,704]{1,0:T(8,128)(2,1)} all-gather(bf16[64,704]{1,0:T(8,128)(2,1)} %param.32), channel_id=1, replica_groups=mesh['sp_0'=8,'sp_1'=4,'tp'=8] {'sp_1'}, dimensions={0}, use_global_device_ids=true | all-gather | bytes 450560 | tf_op jit(solution)/shard_map/all_gather | solution.py:61
  39.8 1.5 copy.610
  42.3 4.2 %fusion.208 = (f32[16,1,512]{2,1,0:T(1,128)}, f32[16,1,512]{2,1,0:T(1,128)}, f32[16,1,512]{2,1,0:T(1,128)}, f32[16,1,512]{2,1,0:T(1,128)}, f32[16,1,512]{2,1,0:T...) fusion(f32[16,16,512]{2,1,0:T(8,128)} %reshape_reshape.16), kind=kLoop, calls=%fused_computation.995 | loop fusion | bytes 1048576 | tf_op jit(solution)/shard_map/slice | solution.py:140
  51.7 1.8 copy_multiply_fusion.1
  69.3 2.2 constant_dynamic-update-slice_fusion.127
  71.5 1.4 constant_dynamic-update-slice_fusion.63
  91.0 1.4 subtract_add_fusion.36
  93.7 1.9 pad.343
  111.8 1.4 constant_dynamic-update-slice_fusion.79
  123.4 1.4 constant_dynamic-update-slice_fusion.62
  124.8 1.4 constant_dynamic-update-slice_fusion.61
  127.5 1.5 constant_dynamic-update-slice_fusion.58
  129.0 1.4 constant_dynamic-update-slice_fusion.57
  130.4 1.4 constant_dynamic-update-slice_fusion.56
  131.9 1.4 constant_dynamic-update-slice_fusion.55
  133.3 1.4 constant_dynamic-update-slice_fusion.54
  134.8 1.4 constant_dynamic-update-slice_fusion.53
  136.2 1.4 constant_dynamic-update-slice_fusion.52
  137.6 1.4 constant_dynamic-update-slice_fusion.51
  147.9 9.8 %all-to-all-start = ((f32[32,6,512]{2,1,0:T(8,128)}), f32[32,6,512]{2,1,0:T(8,128)}, u32[]{:S(2)}, u32[]{:S(2)}) async-start(f32[32,6,512]{2,1,0:T(8,128)} %broadcast_in_dim.148), calls=%async_computation | async-start | bytes 1048576 | tf_op jit(solution)/shard_map/all_to_all | solution.py:17
  157.8 11.6 %all_gather.22 = bf16[704,256]{0,1:T(8,128)(2,1)} all-gather(bf16[704,64]{0,1:T(8,128)(2,1)S(1)} %copy-done.121), channel_id=1, replica_groups=mesh['sp_0'=8,'sp_1'=4,'tp'=8] {'sp_1'}, dimensions={1}, use_global_device_ids=true | all-gather | bytes 450560 | tf_op jit(solution)/shard_map/all_gather | solution.py:61
  170.8 2.2 add.3565
  173.0 2.2 sub.1636
  180.5 1.4 constant_dynamic-update-slice_fusion.125
  181.9 1.4 constant_dynamic-update-slice_fusion.124
  183.3 1.4 constant_dynamic-update-slice_fusion.123
  184.6 1.4 constant_dynamic-update-slice_fusion.122
  187.4 1.4 constant_dynamic-update-slice_fusion.120
  188.7 1.4 constant_dynamic-update-slice_fusion.119
  190.1 1.4 constant_dynamic-update-slice_fusion.118
  191.4 1.4 constant_dynamic-update-slice_fusion.117
  192.8 1.4 constant_dynamic-update-slice_fusion.116
  194.2 1.4 constant_dynamic-update-slice_fusion.115
  195.5 1.4 constant_dynamic-update-slice_fusion.114
  196.9 1.4 constant_dynamic-update-slice_fusion.113
  203.0 1.4 constant_dynamic-update-slice_fusion.64
  205.1 2.5 multiply_add_fusion.2
  216.7 9.6 %all-to-all-start.1 = ((f32[32,6,512]{2,1,0:T(8,128)}), f32[32,6,512]{2,1,0:T(8,128)S(1)}, u32[]{:S(2)}, u32[]{:S(2)}) async-start(f32[32,6,512]{2,1,0:T(8,128)} %broadcast_in_dim.157), calls=%async_computation.1 | async-start | bytes 1048576 | tf_op jit(solution)/shard_map/all_to_all | solution.py:17
  226.3 2.5 fusion.207
  231.4 1.5 fusion.23
  251.8 1.9 multiply_add_fusion.1
  258.7 1.9 multiply_add_fusion
  263.4 28.2 %all_to_all.25 = bf16[8,32,2048]{2,1,0:T(8,128)(2,1)S(1)} all-to-all(bf16[8,32,2048]{2,1,0:T(8,128)(2,1)S(1)} %bitcast.1396), channel_id=1, replica_groups=mesh['sp_0'=8,'sp_1'=4,'tp'=8] {'tp'}, dimensions={0} | all-to-all | bytes 2097152 | tf_op jit(solution)/shard_map/all_to_all | solution.py:72
  292.1 18.4 %all_to_all.26 = bf16[8,32,2048]{2,1,0:T(8,128)(2,1)S(1)} all-to-all(bf16[8,32,2048]{2,1,0:T(8,128)(2,1)S(1)} %broadcast_in_dim.159), channel_id=1, replica_groups=mesh['sp_0'=8,'sp_1'=4,'tp'=8] {'tp'}, dimensions={0} | all-to-all | bytes 2097152 | tf_op jit(solution)/shard_map/all_to_all | solution.py:17
  310.5 4.1 %fusion.216 = f32[256,704]{0,1:T(8,128)} fusion(bf16[256,2048]{1,0:T(8,128)(2,1)S(1)} %bitcast.1409, bf16[2048,704]{1,0:T(8,128)(2,1)} %all-gather.4.cloned.1.call-done), kind=kOutput, calls=%fused_computation.1011 | convolution fusion | flops 738197504 | bytes 4653056 | tf_op jit(solution)/shard_map/dot_general | solution.py:315
  314.6 6.4 %convolution_convert_fusion.1 = bf16[256,2048]{1,0:T(8,128)(2,1)S(1)} fusion(bf16[704,2048]{0,1:T(8,128)(2,1)} %all-gather.8.cloned.1.call-done, bf16[256,2048]{1,0:T(8,128)(2,1)S(1)} %bitcast.1410, bf16[2048,704]{1,0:T(8,128)(2,1)} %all-gather.6.cloned.1.call-done, f32[256,704]{0,1:T(8,128)} %fusion.216), kind=kOutput, calls=%fused_computation.1 | convolution fusion | flops 1478000640 | bytes 8585216 | tf_op jit(solution)/shard_map/dot_general | solution.py:318
  321.0 18.4 %all_to_all.27 = bf16[8,32,2048]{2,1,0:T(8,128)(2,1)S(1)} all-to-all(bf16[8,32,2048]{2,1,0:T(8,128)(2,1)S(1)} %bitcast.1411), channel_id=1, replica_groups=mesh['sp_0'=8,'sp_1'=4,'tp'=8] {'tp'}, dimensions={0} | all-to-all | bytes 2097152 | tf_op jit(solution)/shard_map/all_to_all | solution.py:72
  (829 shorter events, 127.8 us)
Async XLA Ops:
  6.5 256.4 %copy-start = (bf16[128,2048]{1,0:T(8,128)(2,1)S(1)}, bf16[128,2048]{1,0:T(8,128)(2,1)}, u32[]{:S(2)}) copy-start(bf16[128,2048]{1,0:T(8,128)(2,1)} %param.29) | copy-start | bytes 1572868
  6.5 30.0 %copy-start.122 = (s32[256]{0:T(256)S(1)}, s32[256]{0:T(256)}, u32[]{:S(2)}) copy-start(s32[256]{0:T(256)} %param.19) | copy-start | bytes 3076
  6.5 30.1 %copy-start.124 = (f32[8,256]{1,0:T(8,128)S(1)}, f32[8,256]{1,0:T(8,128)}, u32[]{:S(2)}) copy-start(f32[8,256]{1,0:T(8,128)} %param.28) | copy-start | bytes 24580
  6.5 304.0 %all-gather.4.cloned.1.call-start = ((), (), s32[]{:S(2)}) async-start(), calls=%async_computation.5 | async-start | bytes 3538944 | tf_op jit(solution)/shard_map/all_gather | solution.py:61
  19.7 294.9 %all-gather.6.cloned.1.call-start = ((), (), s32[]{:S(2)}) async-start(), calls=%async_computation.6 | async-start | bytes 3538944 | tf_op jit(solution)/shard_map/all_gather | solution.py:61
  53.5 73.3 %copy-start.1 = (f32[16,16,512]{2,0,1:T(8,128)}, f32[16,16,512]{2,0,1:T(8,128)S(1)}, u32[]{:S(2)}) copy-start(f32[16,16,512]{2,0,1:T(8,128)S(1)} %get-tuple-element.523) | copy-start | bytes 1572868
  53.5 73.3 %copy-start.3 = (f32[16,16,512]{2,0,1:T(8,128)}, f32[16,16,512]{2,0,1:T(8,128)S(1)}, u32[]{:S(2)}) copy-start(f32[16,16,512]{2,0,1:T(8,128)S(1)} %get-tuple-element.524) | copy-start | bytes 1572868
  71.4 40.4 %copy-start.37 = (f32[16,1,512]{2,0,1:T(8,128)S(1)}, f32[16,1,512]{2,0,1:T(8,128)}, u32[]{:S(2)}) copy-start(f32[16,1,512]{2,0,1:T(8,128)} %get-tuple-element.147) | copy-start | bytes 98308
  71.4 40.4 %copy-start.38 = (f32[16,1,512]{2,0,1:T(8,128)S(1)}, f32[16,1,512]{2,0,1:T(8,128)}, u32[]{:S(2)}) copy-start(f32[16,1,512]{2,0,1:T(8,128)} %get-tuple-element.220) | copy-start | bytes 98308
  71.4 40.4 %copy-start.39 = (f32[16,1,512]{2,0,1:T(8,128)S(1)}, f32[16,1,512]{2,0,1:T(8,128)}, u32[]{:S(2)}) copy-start(f32[16,1,512]{2,0,1:T(8,128)} %get-tuple-element.221) | copy-start | bytes 98308
  71.5 51.9 %copy-start.54 = (f32[16,1,512]{2,1,0:T(1,128)S(1)}, f32[16,1,512]{2,1,0:T(1,128)}, u32[]{:S(2)}) copy-start(f32[16,1,512]{2,1,0:T(1,128)} %get-tuple-element.314) | copy-start | bytes 98308
  71.5 51.9 %copy-start.56 = (f32[16,1,512]{2,1,0:T(1,128)S(1)}, f32[16,1,512]{2,1,0:T(1,128)}, u32[]{:S(2)}) copy-start(f32[16,1,512]{2,1,0:T(1,128)} %get-tuple-element.329) | copy-start | bytes 98308
  72.9 54.5 %copy-start.83 = (f32[16,1,512]{2,1,0:T(1,128)S(1)}, f32[16,1,512]{2,1,0:T(1,128)}, u32[]{:S(2)}) copy-start(f32[16,1,512]{2,1,0:T(1,128)} %get-tuple-element.310) | copy-start | bytes 98308
  78.4 50.6 %copy-start.79 = (f32[16,1,512]{2,1,0:T(1,128)S(1)}, f32[16,1,512]{2,1,0:T(1,128)}, u32[]{:S(2)}) copy-start(f32[16,1,512]{2,1,0:T(1,128)} %get-tuple-element.309) | copy-start | bytes 98308
  80.5 50.0 %copy-start.75 = (f32[16,1,512]{2,1,0:T(1,128)S(1)}, f32[16,1,512]{2,1,0:T(1,128)}, u32[]{:S(2)}) copy-start(f32[16,1,512]{2,1,0:T(1,128)} %get-tuple-element.308) | copy-start | bytes 98308
  88.4 43.5 %copy-start.71 = (f32[16,1,512]{2,1,0:T(1,128)S(1)}, f32[16,1,512]{2,1,0:T(1,128)}, u32[]{:S(2)}) copy-start(f32[16,1,512]{2,1,0:T(1,128)} %get-tuple-element.307) | copy-start | bytes 98308
  88.4 43.5 %copy-start.81 = (f32[16,1,512]{2,1,0:T(1,128)S(1)}, f32[16,1,512]{2,1,0:T(1,128)}, u32[]{:S(2)}) copy-start(f32[16,1,512]{2,1,0:T(1,128)} %get-tuple-element.322) | copy-start | bytes 98308
  93.7 39.6 %copy-start.67 = (f32[16,1,512]{2,1,0:T(1,128)S(1)}, f32[16,1,512]{2,1,0:T(1,128)}, u32[]{:S(2)}) copy-start(f32[16,1,512]{2,1,0:T(1,128)} %get-tuple-element.306) | copy-start | bytes 98308
  93.7 39.6 %copy-start.77 = (f32[16,1,512]{2,1,0:T(1,128)S(1)}, f32[16,1,512]{2,1,0:T(1,128)}, u32[]{:S(2)}) copy-start(f32[16,1,512]{2,1,0:T(1,128)} %get-tuple-element.321) | copy-start | bytes 98308
  100.2 26.0 %copy-start.91 = (f32[16,1,512]{2,1,0:T(1,128)S(1)}, f32[16,1,512]{2,1,0:T(1,128)}, u32[]{:S(2)}) copy-start(f32[16,1,512]{2,1,0:T(1,128)} %get-tuple-element.312) | copy-start | bytes 98308
  100.2 26.0 %copy-start.98 = (f32[16,1,512]{2,1,0:T(1,128)S(1)}, f32[16,1,512]{2,1,0:T(1,128)}, u32[]{:S(2)}) copy-start(f32[16,1,512]{2,1,0:T(1,128)} %get-tuple-element.327) | copy-start | bytes 98308
  100.2 26.6 %copy-start.87 = (f32[16,1,512]{2,1,0:T(1,128)S(1)}, f32[16,1,512]{2,1,0:T(1,128)}, u32[]{:S(2)}) copy-start(f32[16,1,512]{2,1,0:T(1,128)} %get-tuple-element.311) | copy-start | bytes 98308
  100.2 26.6 %copy-start.96 = (f32[16,1,512]{2,1,0:T(1,128)S(1)}, f32[16,1,512]{2,1,0:T(1,128)}, u32[]{:S(2)}) copy-start(f32[16,1,512]{2,1,0:T(1,128)} %get-tuple-element.326) | copy-start | bytes 98308
  100.2 27.3 %copy-start.93 = (f32[16,1,512]{2,1,0:T(1,128)S(1)}, f32[16,1,512]{2,1,0:T(1,128)}, u32[]{:S(2)}) copy-start(f32[16,1,512]{2,1,0:T(1,128)} %get-tuple-element.325) | copy-start | bytes 98308
  100.2 28.8 %copy-start.89 = (f32[16,1,512]{2,1,0:T(1,128)S(1)}, f32[16,1,512]{2,1,0:T(1,128)}, u32[]{:S(2)}) copy-start(f32[16,1,512]{2,1,0:T(1,128)} %get-tuple-element.324) | copy-start | bytes 98308
  100.2 30.2 %copy-start.85 = (f32[16,1,512]{2,1,0:T(1,128)S(1)}, f32[16,1,512]{2,1,0:T(1,128)}, u32[]{:S(2)}) copy-start(f32[16,1,512]{2,1,0:T(1,128)} %get-tuple-element.323) | copy-start | bytes 98308
  101.1 33.7 %copy-start.63 = (f32[16,1,512]{2,1,0:T(1,128)S(1)}, f32[16,1,512]{2,1,0:T(1,128)}, u32[]{:S(2)}) copy-start(f32[16,1,512]{2,1,0:T(1,128)} %get-tuple-element.305) | copy-start | bytes 98308
  101.1 33.7 %copy-start.73 = (f32[16,1,512]{2,1,0:T(1,128)S(1)}, f32[16,1,512]{2,1,0:T(1,128)}, u32[]{:S(2)}) copy-start(f32[16,1,512]{2,1,0:T(1,128)} %get-tuple-element.320) | copy-start | bytes 98308
  104.9 31.3 %copy-start.61 = (f32[16,1,512]{2,1,0:T(1,128)S(1)}, f32[16,1,512]{2,1,0:T(1,128)}, u32[]{:S(2)}) copy-start(f32[16,1,512]{2,1,0:T(1,128)} %get-tuple-element.304) | copy-start | bytes 98308
  104.9 31.3 %copy-start.69 = (f32[16,1,512]{2,1,0:T(1,128)S(1)}, f32[16,1,512]{2,1,0:T(1,128)}, u32[]{:S(2)}) copy-start(f32[16,1,512]{2,1,0:T(1,128)} %get-tuple-element.319) | copy-start | bytes 98308
  110.3 27.4 %copy-start.59 = (f32[16,1,512]{2,1,0:T(1,128)S(1)}, f32[16,1,512]{2,1,0:T(1,128)}, u32[]{:S(2)}) copy-start(f32[16,1,512]{2,1,0:T(1,128)} %get-tuple-element.303) | copy-start | bytes 98308
  110.3 27.4 %copy-start.65 = (f32[16,1,512]{2,1,0:T(1,128)S(1)}, f32[16,1,512]{2,1,0:T(1,128)}, u32[]{:S(2)}) copy-start(f32[16,1,512]{2,1,0:T(1,128)} %get-tuple-element.318) | copy-start | bytes 98308
  113.2 26.7 %copy-start.13 = (f32[16,16,512]{2,0,1:T(8,128)}, f32[16,16,512]{2,0,1:T(8,128)S(1)}, u32[]{:S(2)}) copy-start(f32[16,16,512]{2,0,1:T(8,128)S(1)} %get-tuple-element.291) | copy-start | bytes 1572868
  113.2 25.9 %copy-start.50 = (f32[16,1,512]{2,1,0:T(1,128)S(1)}, f32[16,1,512]{2,1,0:T(1,128)}, u32[]{:S(2)}) copy-start(f32[16,1,512]{2,1,0:T(1,128)} %get-tuple-element.302) | copy-start | bytes 98308
  113.2 25.9 %copy-start.52 = (f32[16,1,512]{2,1,0:T(1,128)S(1)}, f32[16,1,512]{2,1,0:T(1,128)}, u32[]{:S(2)}) copy-start(f32[16,1,512]{2,1,0:T(1,128)} %get-tuple-element.317) | copy-start | bytes 98308
  147.9 68.0 %all-to-all-start = ((f32[32,6,512]{2,1,0:T(8,128)}), f32[32,6,512]{2,1,0:T(8,128)}, u32[]{:S(2)}, u32[]{:S(2)}) async-start(f32[32,6,512]{2,1,0:T(8,128)} %broadcast_in_dim.148), calls=%async_computation | async-start | bytes 1048576 | tf_op jit(solution)/shard_map/all_to_all | solution.py:17
  157.7 156.8 %all-gather.8.cloned.1.call-start = ((), (), s32[]{:S(2)}) async-start(), calls=%async_computation.7 | async-start | bytes 3538944 | tf_op jit(solution)/shard_map/all_gather | solution.py:61
  176.6 26.2 %copy-start.113 = (f32[16,1,512]{2,0,1:T(8,128)S(1)}, f32[16,1,512]{2,0,1:T(8,128)}, u32[]{:S(2)}) copy-start(f32[16,1,512]{2,0,1:T(8,128)} %get-tuple-element.162) | copy-start | bytes 98308
  176.6 26.2 %copy-start.112 = (f32[16,1,512]{2,0,1:T(8,128)S(1)}, f32[16,1,512]{2,0,1:T(8,128)}, u32[]{:S(2)}) copy-start(f32[16,1,512]{2,0,1:T(8,128)} %get-tuple-element.163) | copy-start | bytes 98308
  176.6 26.3 %copy-start.111 = (f32[16,1,512]{2,0,1:T(8,128)S(1)}, f32[16,1,512]{2,0,1:T(8,128)}, u32[]{:S(2)}) copy-start(f32[16,1,512]{2,0,1:T(8,128)} %get-tuple-element.166) | copy-start | bytes 98308
  176.6 26.3 %copy-start.110 = (f32[16,1,512]{2,0,1:T(8,128)S(1)}, f32[16,1,512]{2,0,1:T(8,128)}, u32[]{:S(2)}) copy-start(f32[16,1,512]{2,0,1:T(8,128)} %get-tuple-element.167) | copy-start | bytes 98308
  176.6 26.3 %copy-start.109 = (f32[16,1,512]{2,0,1:T(8,128)S(1)}, f32[16,1,512]{2,0,1:T(8,128)}, u32[]{:S(2)}) copy-start(f32[16,1,512]{2,0,1:T(8,128)} %get-tuple-element.170) | copy-start | bytes 98308
  176.6 26.3 %copy-start.108 = (f32[16,1,512]{2,0,1:T(8,128)S(1)}, f32[16,1,512]{2,0,1:T(8,128)}, u32[]{:S(2)}) copy-start(f32[16,1,512]{2,0,1:T(8,128)} %get-tuple-element.171) | copy-start | bytes 98308
  176.7 26.3 %copy-start.107 = (f32[16,1,512]{2,0,1:T(8,128)S(1)}, f32[16,1,512]{2,0,1:T(8,128)}, u32[]{:S(2)}) copy-start(f32[16,1,512]{2,0,1:T(8,128)} %get-tuple-element.174) | copy-start | bytes 98308
  176.7 28.4 %copy-start.14 = (f32[16,16,512]{2,0,1:T(8,128)S(1)}, f32[16,16,512]{2,0,1:T(8,128)}, u32[]{:S(2)}) copy-start(f32[16,16,512]{2,0,1:T(8,128)} %copy-done.13) | copy-start | bytes 1572868
  216.7 23.5 %all-to-all-start.1 = ((f32[32,6,512]{2,1,0:T(8,128)}), f32[32,6,512]{2,1,0:T(8,128)S(1)}, u32[]{:S(2)}, u32[]{:S(2)}) async-start(f32[32,6,512]{2,1,0:T(8,128)} %broadcast_in_dim.157), calls=%async_computation.1 | async-start | bytes 1048576 | tf_op jit(solution)/shard_map/all_to_all | solution.py:17
  261.7 30.0 %copy-start.12 = (bf16[32,2048]{1,0:T(8,128)(2,1)S(1)}, bf16[32,2048]{1,0:T(8,128)(2,1)}, u32[]{:S(2)}) copy-start(bf16[32,2048]{1,0:T(8,128)(2,1)} %param.18) | copy-start | bytes 393220
  262.8 29.1 %copy-start.123 = (f32[2048]{0:T(1024)S(1)}, f32[2048]{0:T(1024)}, u32[]{:S(2)}) copy-start(f32[2048]{0:T(1024)} %param.30) | copy-start | bytes 24580
  (87 other events, 444.8 us)
Sparse Core Ops, SparseCore 0:
  19.8 48.4 all-gather.3
  70.1 43.5 all-gather.5
  169.6 53.7 all-gather.7
where the time goes:
time: 353 us; the launch traced here: 347 us
  local copies, waits for them, and re-layouts  120 us (34%)
  blocking collectives  100 us (28%)
  other arithmetic  62.8 us (18%)
  between operations  26.2 us (7%)
  starting transfers between devices  19.5 us (6%)
  matrix products  17.8 us (5%)
    unnamed x330, local copies, waits for them, and re-layouts  49.8 us
    all_to_all x2, blocking collectives, summed_on_arrival(): lax.all_to_all(blocks, axis, split_axis=0, concat_axis=0, tiled=True)  46.6 us
    all_gather x3, blocking collectives, whole_of(): array = lax.all_gather(array, axis, axis=dim, tiled=True)  35.4 us
    unnamed x30, other arithmetic  23.3 us
    all_to_all x2, starting transfers between devices, from_everyone(): return lax.all_to_all(copies, axis, split_axis=0, concat_axis=0, tiled=True)  19.4 us
    all_to_all x1, blocking collectives, from_everyone(): return lax.all_to_all(copies, axis, split_axis=0, concat_axis=0, tiled=True)  18.4 us
    slice x112, local copies, waits for them, and re-layouts, folded_in_pairs(): part[side::2]  11.3 us
    slice x99, local copies, waits for them, and re-layouts, blocked_scan(): outer = lax.associative_scan(pair_combine, ends, reverse=reverse, axis=0)  10.7 us
  transfers between devices with their start and end apart: 5, of which 0 were waited for; matrix products, arithmetic and copies ran while one was open for 55% of the time, Pallas kernels for 0%

commit v1 on v0

v1 whole, which is shorter than its diff:
```python
import functools

import jax
import jax.numpy as jnp
from jax import lax
from jax.experimental import pallas as pl
from jax.experimental.pallas import tpu as pltpu
from jax.sharding import Mesh
from jax.sharding import PartitionSpec as P

HIGHEST = lax.Precision.HIGHEST
MESH = pl.DeviceIdType.MESH
F32, BF16 = jnp.float32, jnp.bfloat16

NZ, NY, NX, NC = 8, 4, 4, 2
SP, TP = NZ * NY, NX * NC
T, CH, G, S, GW = 256, 128, 8, 64, 16
W = G * S
CHUNKS = 8
STEPS = T // CHUNKS
D = 2048
FF = 704
MAIN = 640
ROWS = D // SP
TOK = T // TP
GUA, GUB = MAIN + 128, MAIN
DA, DB = 512, 256
KPAD = DA + DB
NT = (((1,), (1,)), ((), ()))


def dot(a, b, precision=None):
    return jnp.dot(a, b, preferred_element_type=F32, precision=precision)


def dot_nt(a, b, precision=None):
    return lax.dot_general(a, b, NT, preferred_element_type=F32, precision=precision)


def halves(value):
    high = value.astype(BF16)
    return high, (value - high.astype(F32)).astype(BF16)


def iota(shape, dim):
    return lax.broadcasted_iota(jnp.int32, shape, dim)


def one_hot(mask, dtype):
    return jnp.where(mask, 1.0, 0.0).astype(F32).astype(dtype)


def cmul(ar, ai, br, bi):
    return ar * br - ai * bi, ar * bi + ai * br


class Relay:
    def __init__(self, ra, rb, send, recv, base, z, y):
        self.ra, self.rb, self.send, self.recv, self.base = ra, rb, send, recv, base
        self.z, self.y = z, y
        self.started = []

    def zi(self, offset):
        return lax.rem(self.z + (offset + NZ), NZ)

    def yi(self, offset):
        return lax.rem(self.y + (offset + NY), NY)

    def copy(self, number, ref, axis, to):
        to = self.zi(to) if axis == "z" else self.yi(to)
        return pltpu.make_async_remote_copy(
            src_ref=ref,
            dst_ref=ref,
            send_sem=self.send.at[self.base + number],
            recv_sem=self.recv.at[self.base + number],
            device_id={axis: to},
            device_id_type=MESH,
        )

    def start(self, number, ref, axis, to):
        copy = self.copy(number, ref, axis, to)
        copy.start()
        self.started.append(copy)

    def wait(self, number, ref, axis):
        self.copy(number, ref, axis, 1).wait_recv()

    def a_z_ref(self, way, distance):
        ref = self.ra.at[self.zi(-way * distance), self.y]
        return ref

    def a_z_part(self, way, distance, last):
        piece = self.ra.at[self.zi(-way * distance), self.y]
        if last:
            piece = piece.at[pl.ds(0 if way > 0 else ROWS // 2, ROWS // 2)]
        return piece

    def a_send_z(self, d):
        for n, way in enumerate((1, -1)):
            self.start(n * 4 + d - 1, self.a_z_part(way, d - 1, d == 4), "z", way)

    def a_recv_z(self, d):
        for n, way in enumerate((1, -1)):
            self.wait(n * 4 + d - 1, self.a_z_part(way, d, d == 4), "z")

    def a_y(self, offset, dy):
        return self.ra.at[self.zi(offset), self.yi(dy)]

    def a_send_y(self, o):
        q = 8 + 3 * (o % NZ)
        self.start(q, self.a_y(o, 0), "y", 1)
        self.start(q + 1, self.a_y(o, 0), "y", -1)

    def a_pass_y(self, o):
        q = 8 + 3 * (o % NZ)
        self.wait(q, self.a_y(o, -1), "y")
        if o % 2 == 0:
            self.start(q + 2, self.a_y(o, -1), "y", 1)
        self.wait(q + 1, self.a_y(o, 1), "y")
        if o % 2 == 1:
            self.start(q + 2, self.a_y(o, 1), "y", -1)

    def a_last_y(self, o):
        self.wait(8 + 3 * (o % NZ) + 2, self.a_y(o, 2), "y")

    def b_y_part(self, way, distance, last):
        piece = self.rb.at[self.z, self.yi(-way * distance)]
        if last:
            piece = piece.at[pl.ds(0 if way > 0 else ROWS // 2, ROWS // 2)]
        return piece

    def b_send_y(self, d):
        for n, way in enumerate((1, -1)):
            self.start(32 + n * 2 + d - 1, self.b_y_part(way, d - 1, d == 2), "y", way)

    def b_recv_y(self, d):
        for n, way in enumerate((1, -1)):
            self.wait(32 + n * 2 + d - 1, self.b_y_part(way, d, d == 2), "y")

    def b_z_part(self, way, distance, last):
        piece = self.rb.at[self.zi(-way * distance)]
        if last:
            piece = piece.at[pl.ds(0 if way > 0 else NY // 2, NY // 2)]
        return piece

    def b_send_z(self, d):
        for n, way in enumerate((1, -1)):
            self.start(36 + n * 4 + d - 1, self.b_z_part(way, d - 1, d == 4), "z", way)

    def b_recv_z(self, d):
        for n, way in enumerate((1, -1)):
            self.wait(36 + n * 4 + d - 1, self.b_z_part(way, d, d == 4), "z")

    def drain(self):
        for copy in self.started:
            copy.wait_send()


RELAYS = 44
OFFSETS = (0, -1, 1, -2, 2, -3, 3, 4)


def row_of(block):
    return jnp.concatenate([block[g : g + 1, :] for g in range(G)], axis=1)


def rows_of(row):
    return jnp.concatenate([row[:, 128 * k : 128 * (k + 1)] for k in range(W // 128)], axis=0)


def flat_of(rows):
    return jnp.concatenate([rows[k : k + 1, :] for k in range(W // 128)], axis=1)


def kernel(
    mix, stream, docs, doc_scalar, log_dt, decay, freq, in_real, in_imag, out_real, out_imag,
    skip, log_keep, proj, gain, gate_w, up_w, down_w,
    result,
    gua, gub, dna, dnb, drive, factor, states, message, arrived, part, branch, resid, normed,
    hidden, ffn_send, ffn_recv,
    send, recv, carry_send, carry_recv, rs_send, rs_recv, ag_send, ag_recv, fs_send, fs_recv,
):
    z, y, x, c = (lax.axis_index(a) for a in ("z", "y", "x", "c"))
    sp, tp = z * NY + y, x * NC + c

    def sp_peer(k):
        other = lax.rem(sp + k, SP)
        return other, {"z": other // NY, "y": lax.rem(other, NY)}

    def tp_peer(k):
        other = lax.rem(tp + k, TP)
        return other, {"x": other // NC, "c": lax.rem(other, NC)}

    barrier = pltpu.get_barrier_semaphore()

    @pl.loop(1, SP)
    def _(k):
        pl.semaphore_signal(barrier, inc=1, device_id=sp_peer(k)[1], device_id_type=MESH)

    @pl.loop(1, TP)
    def _(k):
        pl.semaphore_signal(barrier, inc=1, device_id=tp_peer(k)[1], device_id_type=MESH)

    gua[z, y, :, 0:MAIN] = up_w[:, 0:MAIN]
    gua[z, y, :, MAIN:GUA] = jnp.concatenate([gate_w[:, MAIN:FF], up_w[:, MAIN:FF]], axis=1)
    gub[z, y] = gate_w[:, 0:MAIN]
    dna[z, y] = down_w[:, 0:DA]
    dnb[z, y] = jnp.concatenate([down_w[:, DA:FF], jnp.zeros((ROWS, KPAD - FF), BF16)], axis=1)

    group = iota((G, S), 0)
    steps = jnp.zeros((G, S), F32)
    for g in range(G):
        steps = jnp.where(group == g, log_dt[g], steps)
    steps = jnp.exp(steps)
    rate, turn_rate = decay[...], freq[...]
    magnitude = jnp.exp(-steps * rate)
    angle = steps * turn_rate
    a_real, a_imag = magnitude * jnp.cos(angle), magnitude * jnp.sin(angle)
    below = rate * rate + turn_rate * turn_rate
    shifted = a_real - 1.0
    z_real = (-shifted * rate + a_imag * turn_rate) / below
    z_imag = (-a_imag * rate - shifted * turn_rate) / below
    ar, ai, zr, zi = (row_of(v) for v in (a_real, a_imag, z_real, z_imag))

    r, t = iota((T, T), 0), iota((T, T), 1)
    order = t == lax.rem(r, CHUNKS) * STEPS + r // CHUNKS
    order_f = one_hot(order, F32)
    u = dot(order_f.astype(BF16), mix[...])
    ub = u.astype(BF16)

    tile = one_hot(lax.rem(iota((S, W), 1), S) == iota((S, W), 0), BF16)
    own = lax.rem(iota((2 * CH, W), 0), CH) // GW == iota((2 * CH, W), 1) // S
    for n, ref in enumerate((in_real, in_imag)):
        high, low = (
            jnp.where(own, dot(half, tile), 0.0).astype(BF16) for half in halves(ref[...])
        )
        for d in range(2):
            at = slice(CH * d, CH * (d + 1))
            drive[:, W * (2 * n + d) : W * (2 * n + d + 1)] = dot(ub, high[at]) + dot(ub, low[at])

    doc = docs[...].astype(F32) + jnp.zeros((G, T), F32)
    place = iota((G, T), 1)
    before, after = pltpu.roll(doc, 1, 1), pltpu.roll(doc, T - 1, 1)
    keep = jnp.exp(log_keep[...])
    keep_f = jnp.where((place == 0) | (doc == before), keep, 0.0)
    keep_b = jnp.where((place == T - 1) | (doc == after), keep, 0.0)
    both = dot_nt(order_f, jnp.concatenate([keep_f, keep_b], axis=0), HIGHEST)
    spread = one_hot(iota((2 * G, 2 * W), 0) == iota((2 * G, 2 * W), 1) // S, F32)
    factor[...] = dot(both, spread, HIGHEST)

    zero = jnp.zeros((CHUNKS, W), F32)
    ar8, ai8 = zero + ar, zero + ai

    def advance(j, state, direction):
        at = pl.ds(pl.multiple_of(j * CHUNKS, CHUNKS), CHUNKS)
        f = factor[at, W * direction : W * (direction + 1)]
        dr = drive[at, W * direction : W * (direction + 1)]
        di = drive[at, W * (2 + direction) : W * (3 + direction)]
        hr, hi = state
        nr, ni = cmul(f * ar8, f * ai8, hr, hi)
        return f, nr + dr, ni + di

    def first(j, state):
        fr, fi, fp, br, bi, bp = state
        f, fr, fi = advance(j, (fr, fi), 0)
        b, br, bi = advance(STEPS - 1 - j, (br, bi), 1)
        return fr, fi, fp * f, br, bi, bp * b

    fr, fi, fp, br, bi, bp = lax.fori_loop(
        0, STEPS, first, (zero, zero, zero + 1.0, zero, zero, zero + 1.0)
    )
    pr, pi = ar, ai
    for _ in range(5):
        pr, pi = cmul(pr, pi, pr, pi)

    def chunk_entries(enter, hr, hi, passed, backward):
        er, ei = enter
        entries = [None] * CHUNKS
        chunks = range(CHUNKS - 1, -1, -1) if backward else range(CHUNKS)
        for k in chunks:
            entries[k] = (er, ei)
            f = passed[k : k + 1]
            nr, ni = cmul(f * pr, f * pi, er, ei)
            er, ei = nr + hr[k : k + 1], ni + hi[k : k + 1]
        return entries, (er, ei)

    none = (jnp.zeros((1, W), F32), jnp.zeros((1, W), F32))
    end_f = chunk_entries(none, fr, fi, fp, False)[1]
    end_b = chunk_entries(none, br, bi, bp, True)[1]
    passed = fp[0:1]
    for k in range(1, CHUNKS):
        passed = passed * fp[k : k + 1]
    qr, qi = pr, pi
    for _ in range(3):
        qr, qi = cmul(qr, qi, qr, qi)
    edge_first = doc_scalar[0].astype(F32)
    edge_last = doc_scalar[T - 1].astype(F32)
    passed_rows = rows_of(passed)
    edges = jnp.concatenate(
        [jnp.full((1, 128), edge_first, F32), jnp.full((1, 128), edge_last, F32),
         jnp.zeros((2, 128), F32)], axis=0)
    for n, (er, ei) in enumerate((end_f, end_b)):
        message[n, 0:4] = rows_of(er)
        message[n, 4:8] = rows_of(ei)
        message[n, 8:12] = passed_rows
        message[n, 12:16] = edges
    arrived[sp] = jnp.zeros((16, 128), F32)

    gu = Relay(gua, gub, send, recv, 0, z, y)
    dn = Relay(dna, dnb, send, recv, RELAYS, z, y)

    pl.semaphore_wait(barrier, SP - 1 + TP - 1)
    gu.a_send_z(1)
    gu.b_send_y(1)
    gu.a_send_y(0)

    def carry_copy(k):
        other, device = sp_peer(k)
        side = jnp.where(other > sp, 0, 1)
        return pltpu.make_async_remote_copy(
            src_ref=message.at[side], dst_ref=arrived.at[sp],
            send_sem=carry_send.at[other], recv_sem=carry_recv.at[sp],
            device_id=device, device_id_type=MESH)

    @pl.loop(1, SP)
    def _(k):
        carry_copy(k).start()

    gu.a_recv_z(1)
    gu.a_send_z(2)
    gu.b_recv_y(1)
    gu.b_send_y(2)
    gu.a_send_y(-1)
    gu.a_send_y(1)
    gu.a_recv_z(2)
    gu.a_send_z(3)
    gu.b_recv_y(2)
    gu.b_send_z(1)
    gu.a_pass_y(0)
    gu.a_send_y(-2)
    gu.a_send_y(2)

    @pl.loop(1, SP)
    def _(k):
        other, device = sp_peer(k)
        pltpu.make_async_remote_copy(
            src_ref=message.at[0], dst_ref=arrived.at[other],
            send_sem=carry_send.at[other], recv_sem=carry_recv.at[other],
            device_id=device, device_id_type=MESH).wait_recv()

    q4r, q4i = rows_of(qr), rows_of(qi)
    four = jnp.zeros((4, 128), F32)

    def fold(j, state, near, far, use):
        cr, ci, last = state
        m = arrived[j]
        link = jnp.where(m[near : near + 1] == last, 1.0, 0.0) * m[8:12]
        nr, ni = cmul(link * q4r, link * q4i, cr, ci)
        cr = jnp.where(use, nr + m[0:4], cr)
        ci = jnp.where(use, ni + m[4:8], ci)
        return cr, ci, jnp.where(use, m[far : far + 1], last)

    def folds(k, state):
        forward = fold(k, state[0], 12, 13, k < sp)
        j = SP - 1 - k
        return forward, fold(j, state[1], 13, 12, j > sp)

    start = (four, four, jnp.zeros((1, 128), F32) - 1.0)
    into_f, into_b = lax.fori_loop(0, SP, folds, (start, start))
    enter_f = jnp.where(into_f[2] == edge_first, 1.0, 0.0)
    enter_b = jnp.where(into_b[2] == edge_last, 1.0, 0.0)
    enter_f = (flat_of(into_f[0] * enter_f), flat_of(into_f[1] * enter_f))
    enter_b = (flat_of(into_b[0] * enter_b), flat_of(into_b[1] * enter_b))
    entries_f = chunk_entries(enter_f, fr, fi, fp, False)[0]
    entries_b = chunk_entries(enter_b, br, bi, bp, True)[0]
    stacked = [
        jnp.concatenate([e[part_no] for e in entries], axis=0)
        for entries in (entries_f, entries_b) for part_no in (0, 1)
    ]

    def second(j, state):
        fr, fi, br, bi = state
        _, fr, fi = advance(j, (fr, fi), 0)
        k = STEPS - 1 - j
        _, br, bi = advance(k, (br, bi), 1)
        at = pl.ds(pl.multiple_of(j * CHUNKS, CHUNKS), CHUNKS)
        states[at, 0:W] = fr
        states[at, 2 * W : 3 * W] = fi
        at = pl.ds(pl.multiple_of(k * CHUNKS, CHUNKS), CHUNKS)
        states[at, W : 2 * W] = br
        states[at, 3 * W : 4 * W] = bi
        return fr, fi, br, bi

    lax.fori_loop(0, STEPS, second, tuple(stacked))

    tile = tile.astype(F32)
    cr = jnp.where(own, dot(out_real[...], tile, HIGHEST), 0.0)
    ci = jnp.where(own, dot(out_imag[...], tile, HIGHEST), 0.0)
    cr, ci = cmul(zr, zi, cr, ci)
    pre = skip[...] * u
    for n in range(4):
        read = (cr if n < 2 else -ci)[CH * (n % 2) : CH * (n % 2 + 1)]
        read_high, read_low = halves(read)
        high, low = halves(states[:, W * n : W * (n + 1)])
        pre = pre + dot_nt(high, read_high) + dot_nt(high, read_low) + dot_nt(low, read_high)
    mixed = jax.nn.gelu(pre).astype(BF16)
    back = one_hot(
        t == lax.rem(r, STEPS) * CHUNKS + r // STEPS, BF16)
    mixed = dot(back, mixed).astype(BF16)
    part[...] = dot(mixed, proj[...]).astype(BF16).reshape(TP, TOK, D)

    def rs_copy(k):
        other, device = tp_peer(k)
        return pltpu.make_async_remote_copy(
            src_ref=part.at[other], dst_ref=branch.at[tp],
            send_sem=rs_send.at[other], recv_sem=rs_recv.at[tp],
            device_id=device, device_id_type=MESH)

    @pl.loop(1, TP)
    def _(k):
        rs_copy(k).start()

    gu.a_recv_z(3)
    gu.a_send_z(4)
    gu.a_send_y(-3)
    gu.a_send_y(3)
    gu.a_pass_y(-1)
    gu.a_pass_y(1)
    dn.a_send_z(1)
    dn.b_send_y(1)
    gu.a_recv_z(4)
    gu.a_send_y(4)
    gu.b_recv_z(1)
    gu.b_send_z(2)
    gu.a_pass_y(-2)
    gu.a_pass_y(2)
    dn.a_send_y(0)
    dn.a_recv_z(1)
    dn.a_send_z(2)
    dn.b_recv_y(1)
    dn.b_send_y(2)

    branch[tp] = part[tp]

    @pl.loop(1, TP)
    def _(k):
        other, device = tp_peer(k)
        pltpu.make_async_remote_copy(
            src_ref=part.at[other], dst_ref=branch.at[other],
            send_sem=rs_send.at[other], recv_sem=rs_recv.at[other],
            device_id=device, device_id_type=MESH).wait_recv()

    kept = stream[...].astype(F32)
    for k in range(TP):
        kept = kept + branch[k].astype(F32)
    resid[...] = kept
    scale = lax.rsqrt(jnp.mean(kept * kept, axis=-1, keepdims=True) + 1e-6)
    normed[tp] = (kept * scale * gain[...]).astype(BF16)

    def ag_copy(k, number):
        other, device = tp_peer(k)
        return pltpu.make_async_remote_copy(
            src_ref=normed.at[number], dst_ref=normed.at[number],
            send_sem=ag_send.at[other], recv_sem=ag_recv.at[number],
            device_id=device, device_id_type=MESH)

    @pl.loop(1, TP)
    def _(k):
        ag_copy(k, tp).start()

    gu.b_recv_z(2)
    gu.b_send_z(3)
    gu.a_pass_y(-3)
    gu.a_pass_y(3)
    dn.a_send_y(-1)
    dn.a_send_y(1)
    dn.a_recv_z(2)
    dn.a_send_z(3)
    dn.b_recv_y(2)
    dn.b_send_z(1)
    dn.a_pass_y(0)
    dn.a_send_y(-2)
    dn.a_send_y(2)
    gu.a_pass_y(4)
    gu.b_recv_z(3)
    gu.b_send_z(4)
    dn.a_recv_z(3)
    dn.a_send_z(4)
    dn.a_send_y(-3)
    dn.a_send_y(3)
    dn.a_pass_y(-1)
    dn.a_pass_y(1)
    dn.a_recv_z(4)
    dn.a_send_y(4)
    for o in OFFSETS:
        gu.a_last_y(o)
    gu.b_recv_z(4)
    dn.b_recv_z(1)
    dn.b_send_z(2)

    @pl.loop(1, TP)
    def _(k):
        other, _ = tp_peer(k)
        ag_copy(k, other).wait_recv()

    rows = normed[...].reshape(T, D)
    second_part = dot(rows, gua[...].reshape(D, GUA))
    first_part = dot(rows, gub[...].reshape(D, GUB))
    hidden[:, 0:MAIN] = (jax.nn.silu(first_part) * second_part[:, 0:MAIN]).astype(BF16)
    tail_gate = second_part[:, MAIN : MAIN + FF - MAIN]
    tail_up = second_part[:, MAIN + FF - MAIN : GUA]
    tail = (jax.nn.silu(tail_gate) * tail_up).astype(BF16)
    hidden[:, MAIN:KPAD] = jnp.concatenate([tail, jnp.zeros((T, KPAD - FF), BF16)], axis=1)

    dn.a_pass_y(-2)
    dn.a_pass_y(2)
    dn.b_recv_z(2)
    dn.b_send_z(3)

    def fs_copy(zi, k, source):
        other, device = tp_peer(k)
        return pltpu.make_async_remote_copy(
            src_ref=ffn_send.at[zi, other], dst_ref=ffn_recv.at[zi, source],
            send_sem=fs_send.at[zi, other], recv_sem=fs_recv.at[zi, source],
            device_id=device, device_id_type=MESH)

    def product(o):
        zi = gu.zi(o)
        out = dot_nt(hidden[:, 0:DA], dna[zi].reshape(NY * ROWS, DA))
        out = out + dot_nt(hidden[:, DA:KPAD], dnb[zi].reshape(NY * ROWS, DB))
        ffn_send[zi] = out.astype(BF16).reshape(TP, TOK, NY * ROWS)

        @pl.loop(1, TP)
        def _(k):
            fs_copy(zi, k, tp).start()

    dn.a_last_y(0)
    product(0)
    dn.a_pass_y(-3)
    dn.a_pass_y(3)
    dn.a_pass_y(4)
    for o in (-1, 1):
        dn.a_last_y(o)
        product(o)
    dn.b_recv_z(3)
    dn.b_send_z(4)
    for o in (-2, 2, -3, 3):
        dn.a_last_y(o)
        product(o)
    dn.b_recv_z(4)
    dn.a_last_y(4)
    product(4)

    for zi in range(NZ):
        @pl.loop(1, TP)
        def _(k):
            other, _ = tp_peer(k)
            fs_copy(zi, k, other).wait_recv()

        at = slice(NY * ROWS * zi, NY * ROWS * (zi + 1))
        ffn_recv[zi, tp] = ffn_send[zi, tp]
        ffn = ffn_recv[zi, 0].astype(F32)
        for k in range(1, TP):
            ffn = ffn + ffn_recv[zi, k].astype(F32)
        result[:, at] = (resid[:, at] + 0.5 * ffn).astype(BF16)

    gu.drain()
    dn.drain()

    @pl.loop(1, SP)
    def _(k):
        carry_copy(k).wait_send()

    @pl.loop(1, TP)
    def _(k):
        rs_copy(k).wait_send()
        ag_copy(k, tp).wait_send()

        @pl.loop(0, NZ)
        def _(zi):
            fs_copy(zi, k, tp).wait_send()


def by_channel(maps):
    return jnp.swapaxes(maps, 2, 3).reshape(2 * CH, S)


def local(
    mix_input, stream, doc_ids, log_dt, decay_rate, frequency, input_real, input_imag,
    output_real, output_imag, skip_gain, log_keep, proj_weight, norm_gain, gate_weight,
    up_weight, down_weight,
):
    vmem = pl.BlockSpec(memory_space=pltpu.VMEM)
    smem = pl.BlockSpec(memory_space=pltpu.SMEM)
    specs = [vmem] * 3 + [smem] * 2 + [vmem] * 13
    dma = pltpu.SemaphoreType.DMA
    scratch = [
        pltpu.VMEM((NZ, NY, ROWS, GUA), BF16),
        pltpu.VMEM((NZ, NY, ROWS, GUB), BF16),
        pltpu.VMEM((NZ, NY, ROWS, DA), BF16),
        pltpu.VMEM((NZ, NY, ROWS, DB), BF16),
        pltpu.VMEM((T, 4 * W), F32),
        pltpu.VMEM((T, 2 * W), F32),
        pltpu.VMEM((T, 4 * W), F32),
        pltpu.VMEM((2, 16, 128), F32),
        pltpu.VMEM((SP, 16, 128), F32),
        pltpu.VMEM((TP, TOK, D), BF16),
        pltpu.VMEM((TP, TOK, D), BF16),
        pltpu.VMEM((TOK, D), F32),
        pltpu.VMEM((TP, TOK, D), BF16),
        pltpu.VMEM((T, KPAD), BF16),
        pltpu.VMEM((NZ, TP, TOK, NY * ROWS), BF16),
        pltpu.VMEM((NZ, TP, TOK, NY * ROWS), BF16),
        dma((2 * RELAYS,)), dma((2 * RELAYS,)),
        dma((SP,)), dma((SP,)),
        dma((TP,)), dma((TP,)),
        dma((TP,)), dma((TP,)),
        dma((NZ, TP)), dma((NZ, TP)),
    ]
    return pl.pallas_call(
        kernel,
        out_shape=jax.ShapeDtypeStruct((TOK, D), BF16),
        in_specs=specs,
        out_specs=vmem,
        scratch_shapes=scratch,
        compiler_params=pltpu.CompilerParams(
            collective_id=0, has_side_effects=True, vmem_limit_bytes=60 << 20
        ),
        name="layer",
    )(
        mix_input, stream, doc_ids.reshape(1, T), doc_ids, log_dt, decay_rate, frequency,
        by_channel(input_real), by_channel(input_imag),
        output_real.reshape(2 * CH, S), output_imag.reshape(2 * CH, S),
        skip_gain.reshape(1, CH), log_keep, proj_weight, norm_gain.reshape(1, D),
        gate_weight, up_weight, down_weight.T,
    )


def solution(mesh):
    torus = Mesh(mesh.devices.reshape(NZ, NY, NX, NC), ("z", "y", "x", "c"))
    sp, tp = ("z", "y"), ("x", "c")
    every = ("z", "y", "x", "c")
    in_specs = (
        P(sp, tp), P(every, None), P(sp), P(tp), P(tp, None), P(tp, None),
        P(None, tp, None, None), P(None, tp, None, None),
        P(None, tp, None, None), P(None, tp, None, None),
        P(tp), P(tp, sp), P(tp, None), P(), P(sp, tp), P(sp, tp), P(tp, sp),
    )
    return jax.shard_map(
        local, mesh=torus, in_specs=in_specs, out_specs=P(every, None), check_vma=False
    )
```

time: 353 us -> 88.1 us (0.25); the launches traced: 347 us -> 88 us
  local copies, waits for them, and re-layouts: 120 us -> 1.57 us
  blocking collectives: 100 us -> 0 us
  Pallas kernels: 0 us -> 86.4 us
  other arithmetic: 62.8 us -> 0 us
  between operations: 26.2 us -> 0.01 us
  starting transfers between devices: 19.5 us -> 0 us
  matrix products: 17.8 us -> 0 us
    pallas_call x0 -> x1, Pallas kernels: none -> 86.4 us  [local(): pl.pallas_call(kernel, out_shape=jax.ShapeDtypeStruct((TOK, D), BF16), in...]
    all_to_all x3 -> x0, blocking collectives: 65 us -> none  [the longest x2 46.6 us: summed_on_arrival(): lax.all_to_all(blocks, axis, split_axis=0, concat_axis=0, tiled=True)]
    unnamed x330 -> x1, local copies, waits for them, and re-layouts: 49.8 us -> 1.57 us
    slice x242 -> x0, local copies, waits for them, and re-layouts: 37.7 us -> none  [the longest x112 11.3 us: folded_in_pairs(): part[side::2]]
    all_gather x3 -> x0, blocking collectives: 35.4 us -> none  [whole_of(): array = lax.all_gather(array, axis, axis=dim, tiled=True)]
    unnamed x30 -> x0, other arithmetic: 23.3 us -> none
    all_to_all x2 -> x0, starting transfers between devices: 19.4 us -> none  [from_everyone(): return lax.all_to_all(copies, axis, split_axis=0, concat_axis=0, tiled=True)]
    add x80 -> x0, other arithmetic: 18.8 us -> none  [the longest x32 5.17 us: blocked_scan(): outer = lax.associative_scan(pair_combine, ends, reverse=reverse, axis=0)]
  transfers between devices with their start and end apart: 5 -> 0, of which waited for: 0 -> 0; matrix products, arithmetic and copies ran while one was open for 55% -> 0% of each run, Pallas kernels for 0% -> 0%
where the time goes in v1:
time: 88.1 us; the launch traced here: 88 us
  Pallas kernels  86.4 us (98%)
  local copies, waits for them, and re-layouts  1.57 us (2%)
    pallas_call x1, Pallas kernels, local(): pl.pallas_call(kernel, out_shape=jax.ShapeDtypeStruct((TOK, D), BF16), in...  86.4 us

profile of v1, /device:TPU:1, one launch (start us, length us, event | category | flops | bytes accessed | tf_op | source)
XLA Modules:
  0.0 88.0 jit_solution(15154090206316447388)
XLA Ops:
  0.0 86.4 %layer.1 = bf16[32,2048]{1,0:T(8,128)(2,1)} custom-call(bf16[256,128]{1,0:T(8,128)(2,1)} %mix.1, bf16[32,2048]{1,0:T(8,128)(2,1)} %stream.1, s32[1,256]{1,0:T(1,128)} %bitcast.18, s32[256]{0:T(256)} %doc_scalar.1, f32[8]{0:T(128)} %log_dt.1, f32[8,64]{1,0:T(8,128)} %decay.1, f32[8,64]{1,0:T(8,128)} %freq.1, f32[256,64]{1,0:T(8,128)} %bitcast.12, ...), custom_call_target="tpu_custom_call" | custom-call | tf_op jit(solution)/shard_map/layer/pallas_call | solution.py:620
  86.4 1.6 %copy.19 = bf16[32,2048]{1,0:T(8,128)(2,1)} copy(bf16[32,2048]{1,0:T(8,128)(2,1)} %layer.1) | data formatting | bytes 262144

commit v2 on v1

v2 whole, which is shorter than its diff:
```python
import functools

import jax
import jax.numpy as jnp
from jax import lax
from jax.experimental import pallas as pl
from jax.experimental.pallas import tpu as pltpu
from jax.sharding import Mesh
from jax.sharding import PartitionSpec as P

HIGHEST = lax.Precision.HIGHEST
MESH = pl.DeviceIdType.MESH
F32, BF16 = jnp.float32, jnp.bfloat16

NZ, NY, NX, NC = 8, 4, 4, 2
SP, TP = NZ * NY, NX * NC
T, CH, G, S, GW = 256, 128, 8, 64, 16
W = G * S
CHUNKS = 8
STEPS = T // CHUNKS
D = 2048
FF = 704
MAIN = 640
ROWS = D // SP
TOK = T // TP
GUA, GUB = MAIN + 128, MAIN
DA, DB = 512, 256
KPAD = DA + DB
NT = (((1,), (1,)), ((), ()))


def dot(a, b, precision=None):
    return jnp.dot(a, b, preferred_element_type=F32, precision=precision)


def dot_nt(a, b, precision=None):
    return lax.dot_general(a, b, NT, preferred_element_type=F32, precision=precision)


def halves(value):
    high = value.astype(BF16)
    return high, (value - high.astype(F32)).astype(BF16)


def iota(shape, dim):
    return lax.broadcasted_iota(jnp.int32, shape, dim)


def one_hot(mask, dtype):
    return jnp.where(mask, 1.0, 0.0).astype(F32).astype(dtype)


def cmul(ar, ai, br, bi):
    return ar * br - ai * bi, ar * bi + ai * br


class Relay:
    def __init__(self, ra, rb, send, recv, z, y):
        self.ra, self.rb, self.send, self.recv = ra, rb, send, recv
        self.z, self.y = z, y

    def zi(self, offset):
        return lax.rem(self.z + (offset + NZ), NZ)

    def yi(self, offset):
        return lax.rem(self.y + (offset + NY), NY)

    def start(self, number, ref, axis, to):
        pltpu.make_async_remote_copy(
            src_ref=ref,
            dst_ref=ref,
            send_sem=self.send.at[0 if number < 20 else 1],
            recv_sem=self.recv.at[number],
            device_id={axis: self.zi(to) if axis == "z" else self.yi(to)},
            device_id_type=MESH,
        ).start()

    def wait(self, number, ref):
        pltpu.make_async_copy(ref, ref, self.recv.at[number]).wait()

    def a(self, dz, dy):
        return self.ra.at[self.zi(dz) * NY + self.yi(dy)]

    def send_az(self, d):
        for way in (1, -1):
            ref = self.a(-way * (d - 1), 0)
            if d == 4:
                ref = ref.at[pl.ds(0 if way > 0 else ROWS // 2, ROWS // 2)]
            self.start(d - 1, ref, "z", way)

    def send_ay(self, o):
        for way in (1, -1):
            self.start(4 + o % NZ, self.a(o, 0), "y", way)

    def az(self, d):
        self.wait(d - 1, self.ra.at[0] if d == 4 else self.ra.at[pl.ds(0, 2)])
        if d < 4:
            self.send_az(d + 1)
        for o in (4,) if d == 4 else (-d, d):
            self.send_ay(o)

    def ay(self, o):
        self.wait(4 + o % NZ, self.ra.at[pl.ds(0, 2)])
        way = 1 if o % 2 == 0 else -1
        self.start(12 + o % NZ, self.a(o, -way), "y", way)

    def al(self, o):
        self.wait(12 + o % NZ, self.ra.at[0])

    def send_by(self, d):
        for way in (1, -1):
            ref = self.rb.at[self.z * NY + self.yi(-way * (d - 1))]
            if d == 2:
                ref = ref.at[pl.ds(0 if way > 0 else ROWS // 2, ROWS // 2)]
            self.start(19 + d, ref, "y", way)

    def by(self, d):
        self.wait(19 + d, self.rb.at[pl.ds(0, 2)] if d == 1 else self.rb.at[0])
        if d == 1:
            self.send_by(2)
        else:
            self.send_bz(1)

    def send_bz(self, d):
        for way in (1, -1):
            first, count = self.zi(-way * (d - 1)) * NY, NY
            if d == 4:
                first, count = first + (0 if way > 0 else NY // 2), NY // 2
            self.start(21 + d, self.rb.at[pl.ds(first, count)], "z", way)

    def bz(self, d):
        self.wait(21 + d, self.rb.at[pl.ds(0, NY if d == 4 else 2 * NY)])
        if d < 4:
            self.send_bz(d + 1)

    def drain(self):
        for n, ref in enumerate((self.ra, self.rb)):
            part = ref.at[pl.ds(0, SP - 1)]
            pltpu.make_async_copy(part, part, self.send.at[n]).wait()


RECVS = 26
OFFSETS = (0, -1, 1, -2, 2, -3, 3, 4)
ORDER = (
    "gby 1", "gaz 1", "line", "gay 0", "gby 2", "gaz 2", "gay -1", "gay 1", "scan", "out",
    "gay -2", "share", "gbz 1", "gay 2", "down", "gaz 3", "dby 1", "pass", "day 0", "gay -3",
    "gbz 2", "daz 1", "gay 3", "dby 2", "last", "gaz 4", "proj", "day -1", "norm", "day 1",
    "gbz 3", "gay 4", "daz 2", "dbz 1", "day -2", "day 2", "gal 0", "gal -1", "gal 1", "gal -2",
    "gal 2", "gal -3", "gal 3", "gal 4", "gbz 4", "widen", "daz 3", "dal 0", "product 0",
    "dal -1", "product -1", "dal 1", "product 1", "dbz 2", "dal -2", "product -2", "dal 2",
    "product 2", "daz 4", "day -3", "day 3", "day 4", "dbz 3", "dal -3", "product -3", "dal 3",
    "product 3", "dbz 4", "dal 4", "product 4", "finish 0", "finish -1", "finish 1", "finish -2",
    "finish 2", "finish -3", "finish 3", "finish 4",
)


def row_of(block):
    return jnp.concatenate([block[g : g + 1, :] for g in range(G)], axis=1)


def rows_of(row):
    return jnp.concatenate([row[:, 128 * k : 128 * (k + 1)] for k in range(W // 128)], axis=0)


def flat_of(rows):
    return jnp.concatenate([rows[k : k + 1, :] for k in range(W // 128)], axis=1)


def kernel(
    mix, stream, docs, doc_scalar, log_dt, decay, freq, in_real, in_imag, out_real, out_imag,
    skip, log_keep, proj, gain, gate_w, up_w, down_w,
    result,
    gua, gub, dna, dnb, drive, factor, states, maps, line, message, column, shared, mixes,
    branch, resid, normed, hidden, ffn_send, ffn_recv,
    gu_send, gu_recv, dn_send, dn_recv, carry_sem, shared_sem, mix_sem, fs_send, fs_recv,
):
    z, y, x, c = (lax.axis_index(a) for a in ("z", "y", "x", "c"))
    sp, tp = z * NY + y, x * NC + c

    def tp_peer(k):
        other = lax.rem(tp + k, TP)
        return other, {"x": other // NC, "c": lax.rem(other, NC)}

    def at_z(k):
        return {"z": lax.rem(z + k, NZ)}

    def at_y(k):
        return {"y": lax.rem(y + k, NY)}

    def at_x(k):
        return {"x": lax.rem(x + k, NX)}

    sibling = {"c": 1 - c}

    barrier = pltpu.get_barrier_semaphore()

    def greet(device):
        pl.semaphore_signal(barrier, inc=1, device_id=device, device_id_type=MESH)

    for k in (1, 7, 2, 6, 3, 5, 4):
        greet(at_z(k))
    for k in (1, 3, 2):
        greet(at_y(k))
    for k in range(1, TP):
        greet(tp_peer(k)[1])

    def push(source, target, sems, n, device):
        pltpu.make_async_remote_copy(
            src_ref=source, dst_ref=target, send_sem=sems.at[0, n], recv_sem=sems.at[1, n],
            device_id=device, device_id_type=MESH).start()

    def take(ref, sem):
        pltpu.make_async_copy(ref, ref, sem).wait()

    gua[sp, :, 0:MAIN] = up_w[:, 0:MAIN]
    gua[sp, :, MAIN:GUA] = jnp.concatenate([gate_w[:, MAIN:FF], up_w[:, MAIN:FF]], axis=1)
    gub[sp] = gate_w[:, 0:MAIN]
    dna[sp] = down_w[:, 0:DA]
    dnb[sp] = jnp.concatenate([down_w[:, DA:FF], jnp.zeros((ROWS, KPAD - FF), BF16)], axis=1)

    shared[tp, 0:CH] = proj[...]
    shared[tp, CH : CH + TOK] = stream[...]

    group = iota((G, S), 0)
    steps = jnp.zeros((G, S), F32)
    for g in range(G):
        steps = jnp.where(group == g, log_dt[g], steps)
    steps = jnp.exp(steps)
    rate, turn_rate = decay[...], freq[...]
    magnitude = jnp.exp(-steps * rate)
    angle = steps * turn_rate
    a_real, a_imag = magnitude * jnp.cos(angle), magnitude * jnp.sin(angle)
    below = rate * rate + turn_rate * turn_rate
    shifted = a_real - 1.0
    z_real = (-shifted * rate + a_imag * turn_rate) / below
    z_imag = (-a_imag * rate - shifted * turn_rate) / below
    ar, ai, zr, zi = (row_of(v) for v in (a_real, a_imag, z_real, z_imag))

    r, t = iota((T, T), 0), iota((T, T), 1)
    order = t == lax.rem(r, CHUNKS) * STEPS + r // CHUNKS
    order_f = one_hot(order, F32)
    u = dot(order_f.astype(BF16), mix[...])
    ub = u.astype(BF16)

    tile = one_hot(lax.rem(iota((S, W), 1), S) == iota((S, W), 0), BF16)
    own = lax.rem(iota((2 * CH, W), 0), CH) // GW == iota((2 * CH, W), 1) // S
    for n, ref in enumerate((in_real, in_imag)):
        high, low = (
            jnp.where(own, dot(half, tile), 0.0).astype(BF16) for half in halves(ref[...])
        )
        for d in range(2):
            at = slice(CH * d, CH * (d + 1))
            drive[:, W * (2 * n + d) : W * (2 * n + d + 1)] = dot(ub, high[at]) + dot(ub, low[at])

    doc = docs[...].astype(F32) + jnp.zeros((G, T), F32)
    place = iota((G, T), 1)
    before, after = pltpu.roll(doc, 1, 1), pltpu.roll(doc, T - 1, 1)
    keep = jnp.exp(log_keep[...])
    keep_f = jnp.where((place == 0) | (doc == before), keep, 0.0)
    keep_b = jnp.where((place == T - 1) | (doc == after), keep, 0.0)
    both = dot_nt(order_f, jnp.concatenate([keep_f, keep_b], axis=0), HIGHEST)
    spread = one_hot(iota((2 * G, 2 * W), 0) == iota((2 * G, 2 * W), 1) // S, F32)
    factor[...] = dot(both, spread, HIGHEST)

    zero = jnp.zeros((CHUNKS, W), F32)
    ar8, ai8 = zero + ar, zero + ai

    def advance(j, state, direction):
        at = pl.ds(pl.multiple_of(j * CHUNKS, CHUNKS), CHUNKS)
        f = factor[at, W * direction : W * (direction + 1)]
        dr = drive[at, W * direction : W * (direction + 1)]
        di = drive[at, W * (2 + direction) : W * (3 + direction)]
        hr, hi = state
        nr, ni = cmul(f * ar8, f * ai8, hr, hi)
        return f, nr + dr, ni + di

    def first(j, state):
        fr, fi, fp, br, bi, bp = state
        f, fr, fi = advance(j, (fr, fi), 0)
        b, br, bi = advance(STEPS - 1 - j, (br, bi), 1)
        return fr, fi, fp * f, br, bi, bp * b

    fr, fi, fp, br, bi, bp = lax.fori_loop(
        0, STEPS, first, (zero, zero, zero + 1.0, zero, zero, zero + 1.0)
    )
    pr, pi = ar, ai
    for _ in range(5):
        pr, pi = cmul(pr, pi, pr, pi)

    def chunk_entries(enter, hr, hi, passed, backward):
        er, ei = enter
        entries = [None] * CHUNKS
        chunks = range(CHUNKS - 1, -1, -1) if backward else range(CHUNKS)
        for k in chunks:
            entries[k] = (er, ei)
            f = passed[k : k + 1]
            nr, ni = cmul(f * pr, f * pi, er, ei)
            er, ei = nr + hr[k : k + 1], ni + hi[k : k + 1]
        return entries, (er, ei)

    none = (jnp.zeros((1, W), F32), jnp.zeros((1, W), F32))
    end_f = chunk_entries(none, fr, fi, fp, False)[1]
    end_b = chunk_entries(none, br, bi, bp, True)[1]
    passed = fp[0:1]
    for k in range(1, CHUNKS):
        passed = passed * fp[k : k + 1]
    qr, qi = pr, pi
    for _ in range(3):
        qr, qi = cmul(qr, qi, qr, qi)
    edge_first = doc_scalar[0].astype(F32)
    edge_last = doc_scalar[T - 1].astype(F32)
    passed_rows = rows_of(passed)
    edges = jnp.concatenate(
        [jnp.full((1, 128), edge_first, F32), jnp.full((1, 128), edge_last, F32),
         jnp.zeros((2, 128), F32)], axis=0)
    for n, (er, ei) in enumerate((end_f, end_b)):
        line[y, 8 * n : 8 * n + 4] = rows_of(er)
        line[y, 8 * n + 4 : 8 * n + 8] = rows_of(ei)
    line[y, 16:20] = passed_rows
    line[y, 20:24] = edges

    gu = Relay(gua, gub, gu_send, gu_recv, z, y)
    dn = Relay(dna, dnb, dn_send, dn_recv, z, y)

    pl.semaphore_wait(barrier, NZ - 1 + NY - 1 + TP - 1)
    gu.send_by(1)
    gu.send_az(1)
    for k in (2, 1, 3):
        push(line.at[y], line.at[y], carry_sem, 0, at_y(k))
    for k in (1, 3):
        push(shared.at[tp], shared.at[tp], shared_sem, 0, at_x(k))
    gu.send_ay(0)
    push(shared.at[tp], shared.at[tp], shared_sem, 2, sibling)

    tile = tile.astype(F32)
    cr = jnp.where(own, dot(out_real[...], tile, HIGHEST), 0.0)
    ci = jnp.where(own, dot(out_imag[...], tile, HIGHEST), 0.0)
    cr, ci = cmul(zr, zi, cr, ci)
    for n in range(4):
        read = (cr if n < 2 else -ci)[CH * (n % 2) : CH * (n % 2 + 1)]
        maps[0, n], maps[1, n] = halves(read)

    q4r, q4i = rows_of(qr), rows_of(qi)
    s4r, s4i = cmul(q4r, q4i, q4r, q4i)
    s4r, s4i = cmul(s4r, s4i, s4r, s4i)
    four = jnp.zeros((4, 128), F32)
    start = (four, four, jnp.zeros((1, 128), F32) - 1.0)

    def fold(state, m, side, power, passed, near, far, use):
        cr, ci, last = state
        link = jnp.where(m[near : near + 1] == last, 1.0, 0.0) * m[passed : passed + 4]
        nr, ni = cmul(link * power[0], link * power[1], cr, ci)
        cr = jnp.where(use, nr + m[side : side + 4], cr)
        ci = jnp.where(use, ni + m[side + 4 : side + 8], ci)
        return cr, ci, jnp.where(use, m[far : far + 1], last)

    def fold_line(state, backward, use):
        for k in range(NY - 1, -1, -1) if backward else range(NY):
            m = line[k]
            if backward:
                state = fold(state, m, 8, (q4r, q4i), 16, 21, 20, use(k))
            else:
                state = fold(state, m, 0, (q4r, q4i), 16, 20, 21, use(k))
        return state

    def carry_line():
        take(line.at[pl.ds(0, NY - 1)], carry_sem.at[1, 0])
        always = lambda k: k >= 0
        ends = fold_line(start, False, always), fold_line(start, True, always)
        passed = line[0][16:20]
        for k in range(1, NY):
            link = jnp.where(line[k][20:21] == line[k - 1][21:22], 1.0, 0.0)
            passed = passed * (link * line[k][16:20])
        edges = jnp.concatenate(
            [line[0][20:21], line[NY - 1][21:22], jnp.zeros((2, 128), F32)], axis=0)
        for n in range(2):
            message[n, 0:4] = ends[n][0]
            message[n, 4:8] = ends[n][1]
            message[n, 8:12] = passed
            message[n, 12:16] = edges
        column[z] = message[0]
        for k in (4, 3, 5, 2, 6, 1, 7):
            side = jnp.where(lax.rem(z + k, NZ) > z, 0, 1)
            push(message.at[side], column.at[z], carry_sem, 1, at_z(k))

    def carry_column():
        take(column.at[pl.ds(0, NZ - 1)], carry_sem.at[1, 1])
        forward, backward = start, start
        for k in range(NZ):
            forward = fold(forward, column[k], 0, (s4r, s4i), 8, 12, 13, k < z)
            j = NZ - 1 - k
            backward = fold(backward, column[j], 0, (s4r, s4i), 8, 13, 12, j > z)
        into_f = fold_line(forward, False, lambda k: k < y)
        into_b = fold_line(backward, True, lambda k: k > y)
        enter_f = jnp.where(into_f[2] == edge_first, 1.0, 0.0)
        enter_b = jnp.where(into_b[2] == edge_last, 1.0, 0.0)
        enter_f = (flat_of(into_f[0] * enter_f), flat_of(into_f[1] * enter_f))
        enter_b = (flat_of(into_b[0] * enter_b), flat_of(into_b[1] * enter_b))
        entries_f = chunk_entries(enter_f, fr, fi, fp, False)[0]
        entries_b = chunk_entries(enter_b, br, bi, bp, True)[0]
        return tuple(
            jnp.concatenate([e[part_no] for e in entries], axis=0)
            for entries in (entries_f, entries_b) for part_no in (0, 1)
        )

    def second(j, state):
        fr, fi, br, bi = state
        _, fr, fi = advance(j, (fr, fi), 0)
        k = STEPS - 1 - j
        _, br, bi = advance(k, (br, bi), 1)
        at = pl.ds(pl.multiple_of(j * CHUNKS, CHUNKS), CHUNKS)
        states[at, 0:W] = fr
        states[at, 2 * W : 3 * W] = fi
        at = pl.ds(pl.multiple_of(k * CHUNKS, CHUNKS), CHUNKS)
        states[at, W : 2 * W] = br
        states[at, 3 * W : 4 * W] = bi
        return fr, fi, br, bi

    def scan():
        lax.fori_loop(0, STEPS, second, carry_column())

    def mix_out():
        pre = skip[...] * u
        for n in range(4):
            high, low = halves(states[:, W * n : W * (n + 1)])
            pre = pre + dot_nt(high, maps[0, n]) + dot_nt(high, maps[1, n])
            pre = pre + dot_nt(low, maps[0, n])
        mixed = jax.nn.gelu(pre).astype(BF16)
        back = one_hot(t == lax.rem(r, STEPS) * CHUNKS + r // STEPS, BF16)
        mixes[tp] = dot(back, mixed).astype(BF16)
        for k in (2, 1, 3):
            push(mixes.at[tp], mixes.at[tp], mix_sem, 0, at_x(k))
        push(mixes.at[tp], mixes.at[tp], mix_sem, 1, sibling)

    def of_x(k):
        return lax.rem(x + k, NX) * NC + c

    def share():
        take(shared.at[pl.ds(0, 2)], shared_sem.at[1, 0])
        half = (CH + TOK) // 2
        for k, first in ((1, half), (3, 0)):
            ref = shared.at[of_x(k), pl.ds(first, half)]
            push(ref, ref, shared_sem, 1, at_x(NX - k))
        for k in (1, 3):
            push(shared.at[of_x(k)], shared.at[of_x(k)], shared_sem, 2, sibling)

    def share_last():
        take(shared.at[0], shared_sem.at[1, 1])
        push(shared.at[of_x(2)], shared.at[of_x(2)], shared_sem, 2, sibling)

    def mix_pass():
        take(mixes.at[pl.ds(0, 3)], mix_sem.at[1, 0])
        for k in (1, 2, 3):
            push(mixes.at[of_x(k)], mixes.at[of_x(k)], mix_sem, 1, sibling)

    def project():
        take(shared.at[pl.ds(0, 4)], shared_sem.at[1, 2])
        take(mixes.at[pl.ds(0, 4)], mix_sem.at[1, 1])
        both = jnp.concatenate([mixes[k] for k in range(TP)], axis=1)
        branch[...] = dot(both, shared[:, 0:CH].reshape(TP * CH, D))

    def normalize():
        scales = gain[...]
        resid[...] = stream[...].astype(F32) + branch[pl.ds(pl.multiple_of(tp * TOK, TOK), TOK)]

        @pl.loop(0, TP)
        def _(k):
            at = pl.ds(pl.multiple_of(k * TOK, TOK), TOK)
            kept = shared[k, CH : CH + TOK].astype(F32) + branch[at]
            scale = lax.rsqrt(jnp.mean(kept * kept, axis=-1, keepdims=True) + 1e-6)
            normed[at] = (kept * scale * scales).astype(BF16)

    def widen():
        rows = normed[...]
        second_part = dot(rows, gua[...].reshape(D, GUA))
        first_part = dot(rows, gub[...].reshape(D, GUB))
        hidden[:, 0:MAIN] = (jax.nn.silu(first_part) * second_part[:, 0:MAIN]).astype(BF16)
        tail_gate = second_part[:, MAIN:FF]
        tail_up = second_part[:, FF:GUA]
        tail = (jax.nn.silu(tail_gate) * tail_up).astype(BF16)
        hidden[:, MAIN:KPAD] = jnp.concatenate([tail, jnp.zeros((T, KPAD - FF), BF16)], axis=1)

    def down_start():
        dn.send_by(1)
        dn.send_az(1)
        dn.send_ay(0)

    def product(o):
        zi = gu.zi(o)
        at = pl.ds(zi * NY, NY)
        out = dot_nt(hidden[:, 0:DA], dna[at].reshape(NY * ROWS, DA))
        out = out + dot_nt(hidden[:, DA:KPAD], dnb[at].reshape(NY * ROWS, DB))
        ffn_send[zi] = out.astype(BF16).reshape(TP, TOK, NY * ROWS)
        ffn_recv[zi, tp] = ffn_send[zi, tp]

        @pl.loop(1, TP)
        def _(k):
            other, device = tp_peer(k)
            pltpu.make_async_remote_copy(
                src_ref=ffn_send.at[zi, other], dst_ref=ffn_recv.at[zi, tp],
                send_sem=fs_send.at[0], recv_sem=fs_recv.at[zi],
                device_id=device, device_id_type=MESH).start()

    def finish(o):
        zi = gu.zi(o)
        take(ffn_recv.at[zi, pl.ds(0, TP - 1)], fs_recv.at[zi])
        at = pl.ds(pl.multiple_of(zi * (NY * ROWS), NY * ROWS), NY * ROWS)
        ffn = ffn_recv[zi, 0].astype(F32)
        for k in range(1, TP):
            ffn = ffn + ffn_recv[zi, k].astype(F32)
        result[:, at] = (resid[:, at] + 0.5 * ffn).astype(BF16)

    steps = {
        "line": carry_line, "scan": scan, "out": mix_out, "share": share, "last": share_last,
        "pass": mix_pass, "proj": project, "norm": normalize, "widen": widen, "down": down_start,
        "product": product, "finish": finish,
    }
    for step in ORDER:
        name, number = step.split()[0], [int(n) for n in step.split()[1:]]
        if name[0] in "gd" and name[1:] in ("az", "ay", "al", "by", "bz"):
            getattr(gu if name[0] == "g" else dn, name[1:])(*number)
        else:
            steps[name](*number)

    gu.drain()
    dn.drain()
    take(line.at[pl.ds(0, NY - 1)], carry_sem.at[0, 0])
    take(column.at[pl.ds(0, NZ - 1)], carry_sem.at[0, 1])
    take(shared.at[pl.ds(0, 2)], shared_sem.at[0, 0])
    take(shared.at[0], shared_sem.at[0, 1])
    take(shared.at[pl.ds(0, 4)], shared_sem.at[0, 2])
    take(mixes.at[pl.ds(0, 3)], mix_sem.at[0, 0])
    take(mixes.at[pl.ds(0, 4)], mix_sem.at[0, 1])
    take(ffn_recv.at[pl.ds(0, TP - 1)], fs_send.at[0])


def by_channel(maps):
    return jnp.swapaxes(maps, 2, 3).reshape(2 * CH, S)


def local(
    mix_input, stream, doc_ids, log_dt, decay_rate, frequency, input_real, input_imag,
    output_real, output_imag, skip_gain, log_keep, proj_weight, norm_gain, gate_weight,
    up_weight, down_weight,
):
    vmem = pl.BlockSpec(memory_space=pltpu.VMEM)
    smem = pl.BlockSpec(memory_space=pltpu.SMEM)
    specs = [vmem] * 3 + [smem] * 2 + [vmem] * 13
    dma = pltpu.SemaphoreType.DMA
    scratch = [
        pltpu.VMEM((SP, ROWS, GUA), BF16),
        pltpu.VMEM((SP, ROWS, GUB), BF16),
        pltpu.VMEM((SP, ROWS, DA), BF16),
        pltpu.VMEM((SP, ROWS, DB), BF16),
        pltpu.VMEM((T, 4 * W), F32),
        pltpu.VMEM((T, 2 * W), F32),
        pltpu.VMEM((T, 4 * W), F32),
        pltpu.VMEM((2, 4, CH, W), BF16),
        pltpu.VMEM((NY, 24, 128), F32),
        pltpu.VMEM((2, 16, 128), F32),
        pltpu.VMEM((NZ, 16, 128), F32),
        pltpu.VMEM((TP, CH + TOK, D), BF16),
        pltpu.VMEM((TP, T, CH), BF16),
        pltpu.VMEM((T, D), F32),
        pltpu.VMEM((TOK, D), F32),
        pltpu.VMEM((T, D), BF16),
        pltpu.VMEM((T, KPAD), BF16),
        pltpu.VMEM((NZ, TP, TOK, NY * ROWS), BF16),
        pltpu.VMEM((NZ, TP, TOK, NY * ROWS), BF16),
        dma((2,)), dma((RECVS,)), dma((2,)), dma((RECVS,)),
        dma((2, 2)), dma((2, 3)), dma((2, 2)), dma((1,)), dma((NZ,)),
    ]
    return pl.pallas_call(
        kernel,
        out_shape=jax.ShapeDtypeStruct((TOK, D), BF16),
        in_specs=specs,
        out_specs=vmem,
        scratch_shapes=scratch,
        compiler_params=pltpu.CompilerParams(
            collective_id=0, has_side_effects=True, vmem_limit_bytes=60 << 20
        ),
        name="layer",
    )(
        mix_input, stream, doc_ids.reshape(1, T), doc_ids, log_dt, decay_rate, frequency,
        by_channel(input_real), by_channel(input_imag),
        output_real.reshape(2 * CH, S), output_imag.reshape(2 * CH, S),
        skip_gain.reshape(1, CH), log_keep, proj_weight, norm_gain.reshape(1, D),
        gate_weight, up_weight, down_weight.T,
    )


def solution(mesh):
    torus = Mesh(mesh.devices.reshape(NZ, NY, NX, NC), ("z", "y", "x", "c"))
    sp, tp = ("z", "y"), ("x", "c")
    every = ("z", "y", "x", "c")
    in_specs = (
        P(sp, tp), P(every, None), P(sp), P(tp), P(tp, None), P(tp, None),
        P(None, tp, None, None), P(None, tp, None, None),
        P(None, tp, None, None), P(None, tp, None, None),
        P(tp), P(tp, sp), P(tp, None), P(), P(sp, tp), P(sp, tp), P(tp, sp),
    )
    return jax.shard_map(
        local, mesh=torus, in_specs=in_specs, out_specs=P(every, None), check_vma=False
    )
```

time: 88.1 us -> 78.4 us (0.89)
  Pallas kernels: 86.4 us -> 76.7 us
    pallas_call x1, Pallas kernels: 86.4 us -> 76.7 us  [local(): pl.pallas_call(kernel, out_shape=jax.ShapeDtypeStruct((TOK, D), BF16), in...]
where the time goes in v2:
time: 78.4 us; the launch traced here: 78.3 us
  Pallas kernels  76.7 us (98%)
  local copies, waits for them, and re-layouts  1.57 us (2%)
    pallas_call x1, Pallas kernels, local(): pl.pallas_call(kernel, out_shape=jax.ShapeDtypeStruct((TOK, D), BF16), in...  76.7 us
    unnamed x1, local copies, waits for them, and re-layouts  1.57 us

profile of v2, /device:TPU:1, one launch (start us, length us, event | category | flops | bytes accessed | tf_op | source)
XLA Modules:
  0.0 78.3 jit_solution(1131331454570625529)
XLA Ops:
  0.0 76.7 %layer.1 = bf16[32,2048]{1,0:T(8,128)(2,1)} custom-call(bf16[256,128]{1,0:T(8,128)(2,1)} %mix.1, bf16[32,2048]{1,0:T(8,128)(2,1)} %stream.1, s32[1,256]{1,0:T(1,128)} %bitcast.18, s32[256]{0:T(256)} %doc_scalar.1, f32[8]{0:T(128)} %log_dt.1, f32[8,64]{1,0:T(8,128)} %decay.1, f32[8,64]{1,0:T(8,128)} %freq.1, f32[256,64]{1,0:T(8,128)} %bitcast.12, ...), custom_call_target="tpu_custom_call" | custom-call | tf_op jit(solution)/shard_map/layer/pallas_call | solution.py:573
  76.7 1.6 %copy.19 = bf16[32,2048]{1,0:T(8,128)(2,1)} copy(bf16[32,2048]{1,0:T(8,128)(2,1)} %layer.1) | data formatting | bytes 262144

commit v3 on v2

--- a/solution.py
+++ b/solution.py
@@ -24,8 +24,9 @@
 ROWS = D // SP
 TOK = T // TP
 GUA, GUB = MAIN + 128, MAIN
-DA, DB = 512, 256
-KPAD = DA + DB
+DA, DB = 512, 128
+DROWS = ROWS + ROWS // 2
+KPAD = MAIN + 256
 NT = (((1,), (1,)), ((), ()))
 
 
@@ -85,7 +86,7 @@
         for way in (1, -1):
             ref = self.a(-way * (d - 1), 0)
             if d == 4:
-                ref = ref.at[pl.ds(0 if way > 0 else ROWS // 2, ROWS // 2)]
+                ref = self.half(ref, way)
             self.start(d - 1, ref, "z", way)
 
     def send_ay(self, o):
@@ -111,27 +112,35 @@
         for way in (1, -1):
             ref = self.rb.at[self.z * NY + self.yi(-way * (d - 1))]
             if d == 2:
-                ref = ref.at[pl.ds(0 if way > 0 else ROWS // 2, ROWS // 2)]
+                ref = self.half(ref, way)
             self.start(19 + d, ref, "y", way)
 
     def by(self, d):
         self.wait(19 + d, self.rb.at[pl.ds(0, 2)] if d == 1 else self.rb.at[0])
         if d == 1:
             self.send_by(2)
-        else:
-            self.send_bz(1)
-
-    def send_bz(self, d):
+        self.send_bz(1, d)
+
+    def send_bz(self, d, j):
         for way in (1, -1):
-            first, count = self.zi(-way * (d - 1)) * NY, NY
-            if d == 4:
-                first, count = first + (0 if way > 0 else NY // 2), NY // 2
-            self.start(21 + d, self.rb.at[pl.ds(first, count)], "z", way)
-
-    def bz(self, d):
-        self.wait(21 + d, self.rb.at[pl.ds(0, NY if d == 4 else 2 * NY)])
+            first = self.zi(-way * (d - 1)) * NY
+            for dy in ((0,), (1, -1), (2,))[j]:
+                if d == 4 and dy == -way:
+                    continue
+                ref = self.rb.at[first + self.yi(dy)]
+                if d == 4 and j != 1:
+                    ref = self.half(ref, way)
+                self.start(19 + 3 * d + j, ref, "z", way)
+
+    def bz(self, d, j):
+        count = (2 if j == 1 else 1) * (1 if d == 4 else 2)
+        self.wait(19 + 3 * d + j, self.rb.at[pl.ds(0, count)])
         if d < 4:
-            self.send_bz(d + 1)
+            self.send_bz(d + 1, j)
+
+    def half(self, ref, way):
+        rows = ref.shape[0] // 2
+        return ref.at[pl.ds(0 if way > 0 else rows, rows)]
 
     def drain(self):
         for n, ref in enumerate((self.ra, self.rb)):
@@ -139,18 +148,21 @@
             pltpu.make_async_copy(part, part, self.send.at[n]).wait()
 
 
-RECVS = 26
+RECVS = 34
 OFFSETS = (0, -1, 1, -2, 2, -3, 3, 4)
 ORDER = (
-    "gby 1", "gaz 1", "line", "gay 0", "gby 2", "gaz 2", "gay -1", "gay 1", "scan", "out",
-    "gay -2", "share", "gbz 1", "gay 2", "down", "gaz 3", "dby 1", "pass", "day 0", "gay -3",
-    "gbz 2", "daz 1", "gay 3", "dby 2", "last", "gaz 4", "proj", "day -1", "norm", "day 1",
-    "gbz 3", "gay 4", "daz 2", "dbz 1", "day -2", "day 2", "gal 0", "gal -1", "gal 1", "gal -2",
-    "gal 2", "gal -3", "gal 3", "gal 4", "gbz 4", "widen", "daz 3", "dal 0", "product 0",
-    "dal -1", "product -1", "dal 1", "product 1", "dbz 2", "dal -2", "product -2", "dal 2",
-    "product 2", "daz 4", "day -3", "day 3", "day 4", "dbz 3", "dal -3", "product -3", "dal 3",
-    "product 3", "dbz 4", "dal 4", "product 4", "finish 0", "finish -1", "finish 1", "finish -2",
-    "finish 2", "finish -3", "finish 3", "finish 4",
+    "maps", "gby 1", "gaz 1", "line", "gbz 1 0", "gay 0", "gby 2", "gbz 1 1", "gay -1", "gaz 2",
+    "gay 1", "downz", "scan", "gbz 2 0", "out", "share", "gbz 1 2", "gay -2", "gay 2", "gbz 2 1",
+    "downy", "gaz 3", "daz 1", "dbz 1 0", "pass", "dby 1", "gbz 3 0", "day 0", "gbz 2 2",
+    "gay -3", "gay 3", "gbz 3 1", "last", "day -1", "gaz 4", "day 1", "daz 2", "dby 2", "proj",
+    "dbz 2 0", "dbz 1 1", "norm", "gbz 3 2", "gay 4", "daz 3", "day -2", "dbz 1 2", "dbz 3 0",
+    "day 2", "dbz 2 1", "gal 0", "gal -1", "gal 1", "gal -2", "gal 2", "gal -3", "gal 3", "gal 4",
+    "gbz 4 0", "gbz 4 1", "gbz 4 2", "widen", "daz 4", "dbz 2 2", "day -3", "dal 0", "product 0",
+    "dal -1", "product -1", "dal 1", "product 1", "day 3", "dbz 3 1", "combine 0", "dal -2",
+    "product -2", "combine -1", "dal 2", "product 2", "combine 1", "combine -2", "dbz 3 2",
+    "combine 2", "day 4", "dal -3", "product -3", "dal 3", "product 3", "combine -3", "combine 3",
+    "dbz 4 0", "dbz 4 1", "dbz 4 2", "dal 4", "product 4", "combine 4", "finish 0", "finish -1",
+    "finish 1", "finish -2", "finish 2", "finish -3", "finish 3", "finish 4",
 )
 
 
@@ -167,12 +179,13 @@
 
 
 def kernel(
-    mix, stream, docs, doc_scalar, log_dt, decay, freq, in_real, in_imag, out_real, out_imag,
-    skip, log_keep, proj, gain, gate_w, up_w, down_w,
+    mix_hbm, stream_hbm, docs, doc_scalar, log_dt, decay, freq, in_real_hbm, in_imag_hbm,
+    out_real_hbm, out_imag_hbm, skip, keep_hbm, proj_hbm, gain, gate_hbm, up_hbm, down_hbm,
     result,
+    mix, stream, in_real, in_imag, out_real, out_imag, log_keep, gate_w, up_w, down_w,
     gua, gub, dna, dnb, drive, factor, states, maps, line, message, column, shared, mixes,
-    branch, resid, normed, hidden, ffn_send, ffn_recv,
-    gu_send, gu_recv, dn_send, dn_recv, carry_sem, shared_sem, mix_sem, fs_send, fs_recv,
+    branch, resid, normed, hidden, ffn_part, ffn_pair, ffn_send, ffn_recv,
+    gu_send, gu_recv, dn_send, dn_recv, carry_sem, shared_sem, mix_sem, pair_sem, fs_send, fs_recv, load_sem,
 ):
     z, y, x, c = (lax.axis_index(a) for a in ("z", "y", "x", "c"))
     sp, tp = z * NY + y, x * NC + c
@@ -212,14 +225,36 @@
     def take(ref, sem):
         pltpu.make_async_copy(ref, ref, sem).wait()
 
-    gua[sp, :, 0:MAIN] = up_w[:, 0:MAIN]
+    loads = []
+
+    def load(source, target):
+        loads.append(pltpu.make_async_copy(source, target, load_sem.at[len(loads)]))
+        loads[-1].start()
+        return loads[-1]
+
+    gate_load = load(gate_hbm, gate_w)
+    up_load = load(up_hbm, up_w)
+    first_loads = [
+        load(gate_hbm.at[:, pl.ds(0, MAIN)], gub.at[sp]),
+        load(up_hbm.at[:, pl.ds(0, MAIN)], gua.at[sp, :, pl.ds(0, MAIN)]),
+    ]
+    scan_loads = [load(mix_hbm, mix), load(keep_hbm, log_keep)]
+    scan_loads += [load(in_real_hbm, in_real), load(in_imag_hbm, in_imag)]
+    share_loads = [
+        load(proj_hbm, shared.at[tp, pl.ds(0, CH)]),
+        load(stream_hbm, shared.at[tp, pl.ds(CH, TOK)]),
+    ]
+    map_loads = [
+        load(out_real_hbm, out_real),
+        load(out_imag_hbm, out_imag),
+        load(stream_hbm, stream),
+        load(down_hbm, down_w),
+        load(down_hbm.at[:, pl.ds(0, DA)], dna.at[sp]),
+        load(down_hbm.at[:, pl.ds(DA, DB)], dnb.at[sp, pl.ds(0, ROWS)]),
+    ]
+    gate_load.wait()
+    up_load.wait()
     gua[sp, :, MAIN:GUA] = jnp.concatenate([gate_w[:, MAIN:FF], up_w[:, MAIN:FF]], axis=1)
-    gub[sp] = gate_w[:, 0:MAIN]
-    dna[sp] = down_w[:, 0:DA]
-    dnb[sp] = jnp.concatenate([down_w[:, DA:FF], jnp.zeros((ROWS, KPAD - FF), BF16)], axis=1)
-
-    shared[tp, 0:CH] = proj[...]
-    shared[tp, CH : CH + TOK] = stream[...]
 
     group = iota((G, S), 0)
     steps = jnp.zeros((G, S), F32)
@@ -235,6 +270,22 @@
     z_real = (-shifted * rate + a_imag * turn_rate) / below
     z_imag = (-a_imag * rate - shifted * turn_rate) / below
     ar, ai, zr, zi = (row_of(v) for v in (a_real, a_imag, z_real, z_imag))
+
+    gu = Relay(gua, gub, gu_send, gu_recv, z, y)
+    dn = Relay(dna, dnb, dn_send, dn_recv, z, y)
+    for wait in first_loads:
+        wait.wait()
+    pl.semaphore_wait(barrier, NZ - 1 + NY - 1 + TP - 1)
+    gu.send_by(1)
+    gu.send_az(1)
+    gu.send_bz(1, 0)
+    for wait in share_loads:
+        wait.wait()
+    for k in (1, 3):
+        push(shared.at[tp], shared.at[tp], shared_sem, 0, at_x(k))
+    push(shared.at[tp], shared.at[tp], shared_sem, 2, sibling)
+    for wait in scan_loads:
+        wait.wait()
 
     r, t = iota((T, T), 0), iota((T, T), 1)
     order = t == lax.rem(r, CHUNKS) * STEPS + r // CHUNKS
@@ -319,26 +370,22 @@
     line[y, 16:20] = passed_rows
     line[y, 20:24] = edges
 
-    gu = Relay(gua, gub, gu_send, gu_recv, z, y)
-    dn = Relay(dna, dnb, dn_send, dn_recv, z, y)
-
-    pl.semaphore_wait(barrier, NZ - 1 + NY - 1 + TP - 1)
-    gu.send_by(1)
-    gu.send_az(1)
     for k in (2, 1, 3):
         push(line.at[y], line.at[y], carry_sem, 0, at_y(k))
-    for k in (1, 3):
-        push(shared.at[tp], shared.at[tp], shared_sem, 0, at_x(k))
     gu.send_ay(0)
-    push(shared.at[tp], shared.at[tp], shared_sem, 2, sibling)
-
-    tile = tile.astype(F32)
-    cr = jnp.where(own, dot(out_real[...], tile, HIGHEST), 0.0)
-    ci = jnp.where(own, dot(out_imag[...], tile, HIGHEST), 0.0)
-    cr, ci = cmul(zr, zi, cr, ci)
-    for n in range(4):
-        read = (cr if n < 2 else -ci)[CH * (n % 2) : CH * (n % 2 + 1)]
-        maps[0, n], maps[1, n] = halves(read)
+
+    def output_maps():
+        for wait in map_loads:
+            wait.wait()
+        spread = tile.astype(F32)
+        cr = jnp.where(own, dot(out_real[...], spread, HIGHEST), 0.0)
+        ci = jnp.where(own, dot(out_imag[...], spread, HIGHEST), 0.0)
+        cr, ci = cmul(zr, zi, cr, ci)
+        for n in range(4):
+            read = (cr if n < 2 else -ci)[CH * (n % 2) : CH * (n % 2 + 1)]
+            maps[0, n], maps[1, n] = halves(read)
+        rest = down_w[:, MAIN:FF]
+        dnb[sp, ROWS:DROWS] = jnp.concatenate([rest[: ROWS // 2], rest[ROWS // 2 :]], axis=1)
 
     q4r, q4i = rows_of(qr), rows_of(qi)
     s4r, s4i = cmul(q4r, q4i, q4r, q4i)
@@ -478,42 +525,61 @@
         tail_gate = second_part[:, MAIN:FF]
         tail_up = second_part[:, FF:GUA]
         tail = (jax.nn.silu(tail_gate) * tail_up).astype(BF16)
-        hidden[:, MAIN:KPAD] = jnp.concatenate([tail, jnp.zeros((T, KPAD - FF), BF16)], axis=1)
-
-    def down_start():
+        empty = jnp.zeros((T, FF - MAIN), BF16)
+        hidden[:, MAIN:KPAD] = jnp.concatenate([tail, empty, empty, tail], axis=1)
+
+    def down_y():
         dn.send_by(1)
+        dn.send_ay(0)
+
+    def down_z():
         dn.send_az(1)
-        dn.send_ay(0)
+        dn.send_bz(1, 0)
 
     def product(o):
         zi = gu.zi(o)
         at = pl.ds(zi * NY, NY)
         out = dot_nt(hidden[:, 0:DA], dna[at].reshape(NY * ROWS, DA))
-        out = out + dot_nt(hidden[:, DA:KPAD], dnb[at].reshape(NY * ROWS, DB))
-        ffn_send[zi] = out.astype(BF16).reshape(TP, TOK, NY * ROWS)
-        ffn_recv[zi, tp] = ffn_send[zi, tp]
-
-        @pl.loop(1, TP)
-        def _(k):
-            other, device = tp_peer(k)
+        out = out + dot_nt(hidden[:, DA:MAIN], dnb[at, 0:ROWS].reshape(NY * ROWS, DB))
+        rest = dnb[at, ROWS:DROWS].reshape(NY * ROWS // 2, DB)
+        sides = [dot_nt(hidden[:, at : at + 128], rest) for at in (MAIN, MAIN + 128)]
+        out = out + jnp.concatenate(
+            [side[:, k : k + ROWS // 2] for k in range(0, 128, ROWS // 2) for side in sides], axis=1
+        )
+        out = out.astype(BF16).reshape(NX, NC, TOK, NY * ROWS)
+        for k in range(NC):
+            ffn_part[zi, k] = out[:, k]
+        pltpu.make_async_remote_copy(
+            src_ref=ffn_part.at[zi, 1 - c], dst_ref=ffn_pair.at[zi],
+            send_sem=fs_send.at[1], recv_sem=pair_sem.at[zi],
+            device_id=sibling, device_id_type=MESH).start()
+
+    def combine(o):
+        zi = gu.zi(o)
+        take(ffn_pair.at[zi], pair_sem.at[zi])
+        total = ffn_part[zi, c].astype(F32) + ffn_pair[zi].astype(F32)
+        ffn_send[zi] = total.astype(BF16)
+        for k in (2, 1, 3):
             pltpu.make_async_remote_copy(
-                src_ref=ffn_send.at[zi, other], dst_ref=ffn_recv.at[zi, tp],
+                src_ref=ffn_send.at[zi, lax.rem(x + k, NX)], dst_ref=ffn_recv.at[zi, x],
                 send_sem=fs_send.at[0], recv_sem=fs_recv.at[zi],
-                device_id=device, device_id_type=MESH).start()
+                device_id=at_x(k), device_id_type=MESH).start()
+        ffn_recv[zi, x] = ffn_send[zi, x]
 
     def finish(o):
         zi = gu.zi(o)
-        take(ffn_recv.at[zi, pl.ds(0, TP - 1)], fs_recv.at[zi])
+        take(ffn_recv.at[zi, pl.ds(0, NX - 1)], fs_recv.at[zi])
         at = pl.ds(pl.multiple_of(zi * (NY * ROWS), NY * ROWS), NY * ROWS)
         ffn = ffn_recv[zi, 0].astype(F32)
-        for k in range(1, TP):
+        for k in range(1, NX):
             ffn = ffn + ffn_recv[zi, k].astype(F32)
         result[:, at] = (resid[:, at] + 0.5 * ffn).astype(BF16)
 
     steps = {
-        "line": carry_line, "scan": scan, "out": mix_out, "share": share, "last": share_last,
-        "pass": mix_pass, "proj": project, "norm": normalize, "widen": widen, "down": down_start,
-        "product": product, "finish": finish,
+        "maps": output_maps, "line": carry_line, "scan": scan, "out": mix_out, "share": share, "last": share_last,
+        "pass": mix_pass, "proj": project, "norm": normalize, "widen": widen, "downz": down_z,
+        "product": product, "combine": combine, "finish": finish,
+        "downy": down_y,
     }
     for step in ORDER:
         name, number = step.split()[0], [int(n) for n in step.split()[1:]]
@@ -531,7 +597,8 @@
     take(shared.at[pl.ds(0, 4)], shared_sem.at[0, 2])
     take(mixes.at[pl.ds(0, 3)], mix_sem.at[0, 0])
     take(mixes.at[pl.ds(0, 4)], mix_sem.at[0, 1])
-    take(ffn_recv.at[pl.ds(0, TP - 1)], fs_send.at[0])
+    take(ffn_recv.at[pl.ds(0, NZ * (NX - 1) // NX)], fs_send.at[0])
+    take(ffn_pair, fs_send.at[1])
 
 
 def by_channel(maps):
@@ -545,13 +612,25 @@
 ):
     vmem = pl.BlockSpec(memory_space=pltpu.VMEM)
     smem = pl.BlockSpec(memory_space=pltpu.SMEM)
-    specs = [vmem] * 3 + [smem] * 2 + [vmem] * 13
+    any_ = pl.BlockSpec(memory_space=pl.ANY)
+    specs = [any_] * 2 + [vmem] + [smem] * 2 + [vmem] * 2 + [any_] * 4 + [vmem] + [any_] * 2
+    specs += [vmem] + [any_] * 3
     dma = pltpu.SemaphoreType.DMA
     scratch = [
+        pltpu.VMEM((T, CH), BF16),
+        pltpu.VMEM((TOK, D), BF16),
+        pltpu.VMEM((2 * CH, S), F32),
+        pltpu.VMEM((2 * CH, S), F32),
+        pltpu.VMEM((2 * CH, S), F32),
+        pltpu.VMEM((2 * CH, S), F32),
+        pltpu.VMEM((G, T), F32),
+        pltpu.VMEM((ROWS, FF), BF16),
+        pltpu.VMEM((ROWS, FF), BF16),
+        pltpu.VMEM((ROWS, FF), BF16),
         pltpu.VMEM((SP, ROWS, GUA), BF16),
         pltpu.VMEM((SP, ROWS, GUB), BF16),
         pltpu.VMEM((SP, ROWS, DA), BF16),
-        pltpu.VMEM((SP, ROWS, DB), BF16),
+        pltpu.VMEM((SP, DROWS, DB), BF16),
         pltpu.VMEM((T, 4 * W), F32),
         pltpu.VMEM((T, 2 * W), F32),
         pltpu.VMEM((T, 4 * W), F32),
@@ -565,14 +644,16 @@
         pltpu.VMEM((TOK, D), F32),
         pltpu.VMEM((T, D), BF16),
         pltpu.VMEM((T, KPAD), BF16),
-        pltpu.VMEM((NZ, TP, TOK, NY * ROWS), BF16),
-        pltpu.VMEM((NZ, TP, TOK, NY * ROWS), BF16),
+        pltpu.VMEM((NZ, NC, NX, TOK, NY * ROWS), BF16),
+        pltpu.VMEM((NZ, NX, TOK, NY * ROWS), BF16),
+        pltpu.VMEM((NZ, NX, TOK, NY * ROWS), BF16),
+        pltpu.VMEM((NZ, NX, TOK, NY * ROWS), BF16),
         dma((2,)), dma((RECVS,)), dma((2,)), dma((RECVS,)),
-        dma((2, 2)), dma((2, 3)), dma((2, 2)), dma((1,)), dma((NZ,)),
+        dma((2, 2)), dma((2, 3)), dma((2, 2)), dma((NZ,)), dma((2,)), dma((NZ,)), dma((16,)),
     ]
     return pl.pallas_call(
         kernel,
-        out_shape=jax.ShapeDtypeStruct((TOK, D), BF16),
+        out_shape=pltpu.VMEM((TOK, D), BF16),
         in_specs=specs,
         out_specs=vmem,
         scratch_shapes=scratch,

time: 78.4 us -> 73.6 us (0.939)
  Pallas kernels: 76.7 us -> 72.8 us
  local copies, waits for them, and re-layouts: 1.57 us -> 0.66 us
    pallas_call x1, Pallas kernels: 76.7 us -> 72.8 us  [local(): pl.pallas_call(kernel, out_shape=pltpu.VMEM((TOK, D), BF16), in_specs=spe...]
    unnamed x1, local copies, waits for them, and re-layouts: 1.57 us -> 0.66 us
where the time goes in v3:
time: 73.6 us; the launch traced here: 73.5 us
  Pallas kernels  72.8 us (99%)
    pallas_call x1, Pallas kernels, local(): pl.pallas_call(kernel, out_shape=pltpu.VMEM((TOK, D), BF16), in_specs=spe...  72.8 us

profile of v3, /device:TPU:1, one launch (start us, length us, event | category | flops | bytes accessed | tf_op | source)
XLA Modules:
  0.0 73.5 jit_solution(6978272119274556694)
XLA Ops:
  0.0 72.8 %layer.1 = bf16[32,2048]{1,0:T(8,128)(2,1)S(1)} custom-call(bf16[256,128]{1,0:T(8,128)(2,1)} %mix_hbm.1, bf16[32,2048]{1,0:T(8,128)(2,1)} %stream_hbm.1, s32[1,256]{1,0:T(1,128)} %bitcast.18, s32[256]{0:T(256)} %doc_scalar.1, f32[8]{0:T(128)} %log_dt.1, f32[8,64]{1,0:T(8,128)} %decay.1, f32[8,64]{1,0:T(8,128)} %freq.1, f32[256,64]{1,0:T(8,128)} %bitcast.12, ...), custom_call_target="tpu_custom_call" | custom-call | tf_op jit(solution)/shard_map/layer/pallas_call | solution.py:654
  72.8 0.7 copy.19

commit v4 on v3

--- a/solution.py
+++ b/solution.py
@@ -56,9 +56,9 @@
 
 
 class Relay:
-    def __init__(self, ra, rb, send, recv, z, y):
+    def __init__(self, ra, rb, send, recv, z, y, joint):
         self.ra, self.rb, self.send, self.recv = ra, rb, send, recv
-        self.z, self.y = z, y
+        self.z, self.y, self.joint = z, y, joint
 
     def zi(self, offset):
         return lax.rem(self.z + (offset + NZ), NZ)
@@ -103,10 +103,13 @@
     def ay(self, o):
         self.wait(4 + o % NZ, self.ra.at[pl.ds(0, 2)])
         way = 1 if o % 2 == 0 else -1
-        self.start(12 + o % NZ, self.a(o, -way), "y", way)
+        self.start(12 + (0 if self.joint else o % NZ), self.a(o, -way), "y", way)
 
     def al(self, o):
         self.wait(12 + o % NZ, self.ra.at[0])
+
+    def all_al(self):
+        self.wait(12, self.ra.at[pl.ds(0, NZ)])
 
     def send_by(self, d):
         for way in (1, -1):
@@ -151,18 +154,18 @@
 RECVS = 34
 OFFSETS = (0, -1, 1, -2, 2, -3, 3, 4)
 ORDER = (
-    "maps", "gby 1", "gaz 1", "line", "gbz 1 0", "gay 0", "gby 2", "gbz 1 1", "gay -1", "gaz 2",
-    "gay 1", "downz", "scan", "gbz 2 0", "out", "share", "gbz 1 2", "gay -2", "gay 2", "gbz 2 1",
-    "downy", "gaz 3", "daz 1", "dbz 1 0", "pass", "dby 1", "gbz 3 0", "day 0", "gbz 2 2",
-    "gay -3", "gay 3", "gbz 3 1", "last", "day -1", "gaz 4", "day 1", "daz 2", "dby 2", "proj",
-    "dbz 2 0", "dbz 1 1", "norm", "gbz 3 2", "gay 4", "daz 3", "day -2", "dbz 1 2", "dbz 3 0",
-    "day 2", "dbz 2 1", "gal 0", "gal -1", "gal 1", "gal -2", "gal 2", "gal -3", "gal 3", "gal 4",
-    "gbz 4 0", "gbz 4 1", "gbz 4 2", "widen", "daz 4", "dbz 2 2", "day -3", "dal 0", "product 0",
-    "dal -1", "product -1", "dal 1", "product 1", "day 3", "dbz 3 1", "combine 0", "dal -2",
-    "product -2", "combine -1", "dal 2", "product 2", "combine 1", "combine -2", "dbz 3 2",
-    "combine 2", "day 4", "dal -3", "product -3", "dal 3", "product 3", "combine -3", "combine 3",
-    "dbz 4 0", "dbz 4 1", "dbz 4 2", "dal 4", "product 4", "combine 4", "finish 0", "finish -1",
-    "finish 1", "finish -2", "finish 2", "finish -3", "finish 3", "finish 4",
+    "maps", "gaz 1", "gby 1", "gbz 1 0", "line", "gay 0", "gay -1", "gaz 2", "gay 1", "gby 2",
+    "gbz 1 1", "gbz 2 0", "gay -2", "scan", "share", "out", "gbz 1 2", "gay 2", "gaz 3",
+    "gbz 2 1", "daz 1", "dbz 1 0", "gbz 3 0", "gay -3", "gbz 2 2", "day 0", "gaz 4", "dby 1",
+    "gay 3", "day -1", "last", "day 1", "gbz 3 1", "daz 2", "dbz 2 0", "pass", "gay 4", "dby 2",
+    "gbz 3 2", "proj", "dbz 1 1", "norm", "day -2", "dbz 3 0", "day 2", "dbz 1 2", "daz 3",
+    "gbz 4 0", "gbz 4 1", "gbz 4 2", "widen", "dal 0", "product 0", "dbz 2 2", "dal 1",
+    "product 1", "daz 4", "dbz 2 1", "dal -2", "product -2", "dal 2", "product 2", "day -3",
+    "combine 0", "dal -1", "product -1", "day 3", "combine -2", "combine 1", "combine 2",
+    "dbz 3 2", "combine -1", "dbz 3 1", "day 4", "dal -3", "product -3", "dal 3", "product 3",
+    "combine -3", "dbz 4 0", "dbz 4 1", "dbz 4 2", "dal 4", "product 4", "combine 3", "combine 4",
+    "finish 0", "finish -2", "finish 1", "finish 2", "finish -1", "finish -3", "finish 3",
+    "finish 4",
 )
 
 
@@ -179,10 +182,11 @@
 
 
 def kernel(
-    mix_hbm, stream_hbm, docs, doc_scalar, log_dt, decay, freq, in_real_hbm, in_imag_hbm,
-    out_real_hbm, out_imag_hbm, skip, keep_hbm, proj_hbm, gain, gate_hbm, up_hbm, down_hbm,
+    mix_hbm, stream_hbm, docs_hbm, log_dt_hbm, decay_hbm, freq_hbm, in_real_hbm, in_imag_hbm,
+    out_real_hbm, out_imag_hbm, skip_hbm, keep_hbm, proj_hbm, gain_hbm, gate_hbm, up_hbm, down_hbm,
     result,
-    mix, stream, in_real, in_imag, out_real, out_imag, log_keep, gate_w, up_w, down_w,
+    mix, stream, docs, log_dt, decay, freq, in_real, in_imag, out_real, out_imag, skip, log_keep,
+    gain, gate_w, up_w, down_w,
     gua, gub, dna, dnb, drive, factor, states, maps, line, message, column, shared, mixes,
     branch, resid, normed, hidden, ffn_part, ffn_pair, ffn_send, ffn_recv,
     gu_send, gu_recv, dn_send, dn_recv, carry_sem, shared_sem, mix_sem, pair_sem, fs_send, fs_recv, load_sem,
@@ -225,41 +229,74 @@
     def take(ref, sem):
         pltpu.make_async_copy(ref, ref, sem).wait()
 
-    loads = []
-
-    def load(source, target):
-        loads.append(pltpu.make_async_copy(source, target, load_sem.at[len(loads)]))
-        loads[-1].start()
-        return loads[-1]
-
-    gate_load = load(gate_hbm, gate_w)
-    up_load = load(up_hbm, up_w)
-    first_loads = [
-        load(gate_hbm.at[:, pl.ds(0, MAIN)], gub.at[sp]),
-        load(up_hbm.at[:, pl.ds(0, MAIN)], gua.at[sp, :, pl.ds(0, MAIN)]),
+    def load(n, *pairs):
+        copies = [pltpu.make_async_copy(*pair, load_sem.at[n]) for pair in pairs]
+        for copy in copies:
+            copy.start()
+        return copies
+
+    def loaded(copies):
+        for copy in copies:
+            copy.wait()
+
+    gate_load = load(0, (gate_hbm, gate_w))
+    up_load = load(1, (up_hbm, up_w))
+    gate_piece = load(2, (gate_hbm.at[:, pl.ds(0, MAIN)], gub.at[sp]))
+    up_piece = load(3, (up_hbm.at[:, pl.ds(0, MAIN)], gua.at[sp, :, pl.ds(0, MAIN)]))
+    down_load = load(17, (down_hbm, down_w))
+    down_pieces = [
+        load(18, (down_hbm.at[:, pl.ds(0, DA)], dna.at[sp])),
+        load(19, (down_hbm.at[:, pl.ds(DA, DB)], dnb.at[sp, pl.ds(0, ROWS)])),
     ]
-    scan_loads = [load(mix_hbm, mix), load(keep_hbm, log_keep)]
-    scan_loads += [load(in_real_hbm, in_real), load(in_imag_hbm, in_imag)]
+    scan_loads = [
+        load(4 + n, pair) for n, pair in enumerate((
+            (log_dt_hbm, log_dt), (decay_hbm, decay), (freq_hbm, freq), (mix_hbm, mix),
+            (docs_hbm, docs), (keep_hbm, log_keep), (in_real_hbm, in_real), (in_imag_hbm, in_imag),
+        ))
+    ]
     share_loads = [
-        load(proj_hbm, shared.at[tp, pl.ds(0, CH)]),
-        load(stream_hbm, shared.at[tp, pl.ds(CH, TOK)]),
+        load(12, (proj_hbm, shared.at[tp, pl.ds(0, CH)])),
+        load(13, (stream_hbm, shared.at[tp, pl.ds(CH, TOK)])),
     ]
     map_loads = [
-        load(out_real_hbm, out_real),
-        load(out_imag_hbm, out_imag),
-        load(stream_hbm, stream),
-        load(down_hbm, down_w),
-        load(down_hbm.at[:, pl.ds(0, DA)], dna.at[sp]),
-        load(down_hbm.at[:, pl.ds(DA, DB)], dnb.at[sp, pl.ds(0, ROWS)]),
+        load(n, pair) for n, pair in (
+            (14, (out_real_hbm, out_real)), (15, (out_imag_hbm, out_imag)),
+            (16, (stream_hbm, stream)), (20, (skip_hbm, skip)), (21, (gain_hbm, gain)),
+        )
     ]
-    gate_load.wait()
-    up_load.wait()
+    loaded(gate_load)
+    loaded(up_load)
     gua[sp, :, MAIN:GUA] = jnp.concatenate([gate_w[:, MAIN:FF], up_w[:, MAIN:FF]], axis=1)
+    loaded(down_load)
+    rest = down_w[:, MAIN:FF]
+    dnb[sp, ROWS:DROWS] = jnp.concatenate([rest[: ROWS // 2], rest[ROWS // 2 :]], axis=1)
+
+    gu = Relay(gua, gub, gu_send, gu_recv, z, y, True)
+    dn = Relay(dna, dnb, dn_send, dn_recv, z, y, False)
+    loaded(gate_piece)
+    loaded(up_piece)
+    pl.semaphore_wait(barrier, NZ - 1 + NY - 1 + TP - 1)
+    gu.send_by(1)
+    gu.send_bz(1, 0)
+    gu.send_az(1)
+    for copies in down_pieces:
+        loaded(copies)
+    dn.send_by(1)
+    dn.send_ay(0)
+    dn.send_az(1)
+    dn.send_bz(1, 0)
+    for copies in share_loads:
+        loaded(copies)
+    for k in (1, 3):
+        push(shared.at[tp], shared.at[tp], shared_sem, 0, at_x(k))
+    push(shared.at[tp], shared.at[tp], shared_sem, 2, sibling)
+    for copies in scan_loads:
+        loaded(copies)
 
     group = iota((G, S), 0)
     steps = jnp.zeros((G, S), F32)
     for g in range(G):
-        steps = jnp.where(group == g, log_dt[g], steps)
+        steps = jnp.where(group == g, log_dt[0:1, g : g + 1], steps)
     steps = jnp.exp(steps)
     rate, turn_rate = decay[...], freq[...]
     magnitude = jnp.exp(-steps * rate)
@@ -271,22 +308,6 @@
     z_imag = (-a_imag * rate - shifted * turn_rate) / below
     ar, ai, zr, zi = (row_of(v) for v in (a_real, a_imag, z_real, z_imag))
 
-    gu = Relay(gua, gub, gu_send, gu_recv, z, y)
-    dn = Relay(dna, dnb, dn_send, dn_recv, z, y)
-    for wait in first_loads:
-        wait.wait()
-    pl.semaphore_wait(barrier, NZ - 1 + NY - 1 + TP - 1)
-    gu.send_by(1)
-    gu.send_az(1)
-    gu.send_bz(1, 0)
-    for wait in share_loads:
-        wait.wait()
-    for k in (1, 3):
-        push(shared.at[tp], shared.at[tp], shared_sem, 0, at_x(k))
-    push(shared.at[tp], shared.at[tp], shared_sem, 2, sibling)
-    for wait in scan_loads:
-        wait.wait()
-
     r, t = iota((T, T), 0), iota((T, T), 1)
     order = t == lax.rem(r, CHUNKS) * STEPS + r // CHUNKS
     order_f = one_hot(order, F32)
@@ -358,12 +379,11 @@
     qr, qi = pr, pi
     for _ in range(3):
         qr, qi = cmul(qr, qi, qr, qi)
-    edge_first = doc_scalar[0].astype(F32)
-    edge_last = doc_scalar[T - 1].astype(F32)
+    edge_first = jnp.broadcast_to(doc[0:1, 0:1], (1, 128))
+    edge_last = jnp.broadcast_to(doc[0:1, T - 1 : T], (1, 128))
     passed_rows = rows_of(passed)
     edges = jnp.concatenate(
-        [jnp.full((1, 128), edge_first, F32), jnp.full((1, 128), edge_last, F32),
-         jnp.zeros((2, 128), F32)], axis=0)
+        [edge_first, edge_last, jnp.zeros((2, 128), F32)], axis=0)
     for n, (er, ei) in enumerate((end_f, end_b)):
         line[y, 8 * n : 8 * n + 4] = rows_of(er)
         line[y, 8 * n + 4 : 8 * n + 8] = rows_of(ei)
@@ -375,8 +395,8 @@
     gu.send_ay(0)
 
     def output_maps():
-        for wait in map_loads:
-            wait.wait()
+        for copies in map_loads:
+            loaded(copies)
         spread = tile.astype(F32)
         cr = jnp.where(own, dot(out_real[...], spread, HIGHEST), 0.0)
         ci = jnp.where(own, dot(out_imag[...], spread, HIGHEST), 0.0)
@@ -384,8 +404,6 @@
         for n in range(4):
             read = (cr if n < 2 else -ci)[CH * (n % 2) : CH * (n % 2 + 1)]
             maps[0, n], maps[1, n] = halves(read)
-        rest = down_w[:, MAIN:FF]
-        dnb[sp, ROWS:DROWS] = jnp.concatenate([rest[: ROWS // 2], rest[ROWS // 2 :]], axis=1)
 
     q4r, q4i = rows_of(qr), rows_of(qi)
     s4r, s4i = cmul(q4r, q4i, q4r, q4i)
@@ -518,6 +536,7 @@
             normed[at] = (kept * scale * scales).astype(BF16)
 
     def widen():
+        gu.all_al()
         rows = normed[...]
         second_part = dot(rows, gua[...].reshape(D, GUA))
         first_part = dot(rows, gub[...].reshape(D, GUB))
@@ -527,14 +546,6 @@
         tail = (jax.nn.silu(tail_gate) * tail_up).astype(BF16)
         empty = jnp.zeros((T, FF - MAIN), BF16)
         hidden[:, MAIN:KPAD] = jnp.concatenate([tail, empty, empty, tail], axis=1)
-
-    def down_y():
-        dn.send_by(1)
-        dn.send_ay(0)
-
-    def down_z():
-        dn.send_az(1)
-        dn.send_bz(1, 0)
 
     def product(o):
         zi = gu.zi(o)
@@ -577,9 +588,9 @@
 
     steps = {
         "maps": output_maps, "line": carry_line, "scan": scan, "out": mix_out, "share": share, "last": share_last,
-        "pass": mix_pass, "proj": project, "norm": normalize, "widen": widen, "downz": down_z,
+        "pass": mix_pass, "proj": project, "norm": normalize, "widen": widen,
         "product": product, "combine": combine, "finish": finish,
-        "downy": down_y,
+
     }
     for step in ORDER:
         name, number = step.split()[0], [int(n) for n in step.split()[1:]]
@@ -611,19 +622,22 @@
     up_weight, down_weight,
 ):
     vmem = pl.BlockSpec(memory_space=pltpu.VMEM)
-    smem = pl.BlockSpec(memory_space=pltpu.SMEM)
-    any_ = pl.BlockSpec(memory_space=pl.ANY)
-    specs = [any_] * 2 + [vmem] + [smem] * 2 + [vmem] * 2 + [any_] * 4 + [vmem] + [any_] * 2
-    specs += [vmem] + [any_] * 3
+    specs = [pl.BlockSpec(memory_space=pl.ANY)] * 17
     dma = pltpu.SemaphoreType.DMA
     scratch = [
         pltpu.VMEM((T, CH), BF16),
         pltpu.VMEM((TOK, D), BF16),
+        pltpu.VMEM((1, T), jnp.int32),
+        pltpu.VMEM((1, G), F32),
+        pltpu.VMEM((G, S), F32),
+        pltpu.VMEM((G, S), F32),
         pltpu.VMEM((2 * CH, S), F32),
         pltpu.VMEM((2 * CH, S), F32),
         pltpu.VMEM((2 * CH, S), F32),
         pltpu.VMEM((2 * CH, S), F32),
+        pltpu.VMEM((1, CH), F32),
         pltpu.VMEM((G, T), F32),
+        pltpu.VMEM((1, D), F32),
         pltpu.VMEM((ROWS, FF), BF16),
         pltpu.VMEM((ROWS, FF), BF16),
         pltpu.VMEM((ROWS, FF), BF16),
@@ -649,7 +663,7 @@
         pltpu.VMEM((NZ, NX, TOK, NY * ROWS), BF16),
         pltpu.VMEM((NZ, NX, TOK, NY * ROWS), BF16),
         dma((2,)), dma((RECVS,)), dma((2,)), dma((RECVS,)),
-        dma((2, 2)), dma((2, 3)), dma((2, 2)), dma((NZ,)), dma((2,)), dma((NZ,)), dma((16,)),
+        dma((2, 2)), dma((2, 3)), dma((2, 2)), dma((NZ,)), dma((2,)), dma((NZ,)), dma((22,)),
     ]
     return pl.pallas_call(
         kernel,
@@ -662,7 +676,7 @@
         ),
         name="layer",
     )(
-        mix_input, stream, doc_ids.reshape(1, T), doc_ids, log_dt, decay_rate, frequency,
+        mix_input, stream, doc_ids.reshape(1, T), log_dt.reshape(1, G), decay_rate, frequency,
         by_channel(input_real), by_channel(input_imag),
         output_real.reshape(2 * CH, S), output_imag.reshape(2 * CH, S),
         skip_gain.reshape(1, CH), log_keep, proj_weight, norm_gain.reshape(1, D),

time: 73.6 us -> 71.8 us (0.976)
  Pallas kernels: 72.8 us -> 71.1 us
    pallas_call x1, Pallas kernels: 72.8 us -> 71.1 us  [local(): pl.pallas_call(kernel, out_shape=pltpu.VMEM((TOK, D), BF16), in_specs=spe...]
where the time goes in v4:
time: 71.8 us; the launch traced here: 71.7 us
  Pallas kernels  71.1 us (99%)
    pallas_call x1, Pallas kernels, local(): pl.pallas_call(kernel, out_shape=pltpu.VMEM((TOK, D), BF16), in_specs=spe...  71.1 us

profile of v4, /device:TPU:1, one launch (start us, length us, event | category | flops | bytes accessed | tf_op | source)
XLA Modules:
  0.0 71.7 jit_solution(3125448790799123948)
XLA Ops:
  0.0 71.1 %layer.1 = bf16[32,2048]{1,0:T(8,128)(2,1)S(1)} custom-call(bf16[256,128]{1,0:T(8,128)(2,1)} %mix_hbm.1, bf16[32,2048]{1,0:T(8,128)(2,1)} %stream_hbm.1, s32[1,256]{1,0:T(1,128)} %bitcast.19, f32[1,8]{1,0:T(1,128)} %bitcast.20, f32[8,64]{1,0:T(8,128)} %decay_hbm.1, f32[8,64]{1,0:T(8,128)} %freq_hbm.1, f32[256,64]{1,0:T(8,128)} %bitcast.13, ...), custom_call_target="tpu_custom_call" | custom-call | tf_op jit(solution)/shard_map/layer/pallas_call | solution.py:668
  71.1 0.7 copy.19

commit v5 on v4

--- a/solution.py
+++ b/solution.py
@@ -154,18 +154,17 @@
 RECVS = 34
 OFFSETS = (0, -1, 1, -2, 2, -3, 3, 4)
 ORDER = (
-    "maps", "gaz 1", "gby 1", "gbz 1 0", "line", "gay 0", "gay -1", "gaz 2", "gay 1", "gby 2",
-    "gbz 1 1", "gbz 2 0", "gay -2", "scan", "share", "out", "gbz 1 2", "gay 2", "gaz 3",
-    "gbz 2 1", "daz 1", "dbz 1 0", "gbz 3 0", "gay -3", "gbz 2 2", "day 0", "gaz 4", "dby 1",
-    "gay 3", "day -1", "last", "day 1", "gbz 3 1", "daz 2", "dbz 2 0", "pass", "gay 4", "dby 2",
-    "gbz 3 2", "proj", "dbz 1 1", "norm", "day -2", "dbz 3 0", "day 2", "dbz 1 2", "daz 3",
-    "gbz 4 0", "gbz 4 1", "gbz 4 2", "widen", "dal 0", "product 0", "dbz 2 2", "dal 1",
-    "product 1", "daz 4", "dbz 2 1", "dal -2", "product -2", "dal 2", "product 2", "day -3",
-    "combine 0", "dal -1", "product -1", "day 3", "combine -2", "combine 1", "combine 2",
-    "dbz 3 2", "combine -1", "dbz 3 1", "day 4", "dal -3", "product -3", "dal 3", "product 3",
-    "combine -3", "dbz 4 0", "dbz 4 1", "dbz 4 2", "dal 4", "product 4", "combine 3", "combine 4",
-    "finish 0", "finish -2", "finish 1", "finish 2", "finish -1", "finish -3", "finish 3",
-    "finish 4",
+    "maps", "gaz 1", "gby 1", "line", "gbz 1 0", "gay 0", "gay -1", "gaz 2", "share", "gay 1",
+    "gby 2", "gbz 1 1", "gbz 2 0", "scan", "out", "share2", "gay 2", "gaz 3", "gay -2", "gbz 1 2",
+    "dbz 1 0", "daz 1", "last", "gbz 2 1", "gay -3", "gbz 3 0", "gaz 4", "gay 3", "gbz 2 2",
+    "dby 1", "pass", "dbz 2 0", "day 0", "day -1", "proj", "day 1", "daz 2", "norm", "gbz 3 1",
+    "gay 4", "dby 2", "gbz 3 2", "dbz 1 1", "dbz 3 0", "day -2", "daz 3", "day 2", "dbz 1 2",
+    "gbz 4 0", "gbz 4 1", "gbz 4 2", "widen", "dal 1", "product 1", "dbz 2 1", "daz 4", "day -3",
+    "day 3", "dbz 2 2", "dal -2", "product -2", "dal -1", "product -1", "combine 1", "dal 2",
+    "product 2", "combine -2", "dal 0", "product 0", "combine -1", "combine 2", "dbz 3 1",
+    "combine 0", "day 4", "dbz 3 2", "dal -3", "product -3", "dal 3", "product 3", "combine -3",
+    "combine 3", "dbz 4 0", "dbz 4 1", "dbz 4 2", "dal 4", "product 4", "combine 4", "finish 1",
+    "finish -2", "finish -1", "finish 2", "finish 0", "finish -3", "finish 3", "finish 4",
 )
 
 
@@ -287,8 +286,11 @@
     dn.send_bz(1, 0)
     for copies in share_loads:
         loaded(copies)
-    for k in (1, 3):
-        push(shared.at[tp], shared.at[tp], shared_sem, 0, at_x(k))
+    half = (CH + TOK) // 2
+    for n, rows in ((0, (0, half)), (3, (half, 0))):
+        for k, first in zip((1, 3), rows):
+            ref = shared.at[tp, pl.ds(first, half)]
+            push(ref, ref, shared_sem, n, at_x(k))
     push(shared.at[tp], shared.at[tp], shared_sem, 2, sibling)
     for copies in scan_loads:
         loaded(copies)
@@ -501,11 +503,13 @@
         return lax.rem(x + k, NX) * NC + c
 
     def share():
-        take(shared.at[pl.ds(0, 2)], shared_sem.at[1, 0])
-        half = (CH + TOK) // 2
+        take(shared.at[0], shared_sem.at[1, 0])
         for k, first in ((1, half), (3, 0)):
             ref = shared.at[of_x(k), pl.ds(first, half)]
             push(ref, ref, shared_sem, 1, at_x(NX - k))
+
+    def share_rest():
+        take(shared.at[0], shared_sem.at[1, 3])
         for k in (1, 3):
             push(shared.at[of_x(k)], shared.at[of_x(k)], shared_sem, 2, sibling)
 
@@ -587,10 +591,10 @@
         result[:, at] = (resid[:, at] + 0.5 * ffn).astype(BF16)
 
     steps = {
-        "maps": output_maps, "line": carry_line, "scan": scan, "out": mix_out, "share": share, "last": share_last,
+        "maps": output_maps, "line": carry_line, "scan": scan, "out": mix_out, "share": share,
+        "share2": share_rest, "last": share_last,
         "pass": mix_pass, "proj": project, "norm": normalize, "widen": widen,
         "product": product, "combine": combine, "finish": finish,
-
     }
     for step in ORDER:
         name, number = step.split()[0], [int(n) for n in step.split()[1:]]
@@ -603,7 +607,8 @@
     dn.drain()
     take(line.at[pl.ds(0, NY - 1)], carry_sem.at[0, 0])
     take(column.at[pl.ds(0, NZ - 1)], carry_sem.at[0, 1])
-    take(shared.at[pl.ds(0, 2)], shared_sem.at[0, 0])
+    take(shared.at[0], shared_sem.at[0, 0])
+    take(shared.at[0], shared_sem.at[0, 3])
     take(shared.at[0], shared_sem.at[0, 1])
     take(shared.at[pl.ds(0, 4)], shared_sem.at[0, 2])
     take(mixes.at[pl.ds(0, 3)], mix_sem.at[0, 0])
@@ -663,7 +668,7 @@
         pltpu.VMEM((NZ, NX, TOK, NY * ROWS), BF16),
         pltpu.VMEM((NZ, NX, TOK, NY * ROWS), BF16),
         dma((2,)), dma((RECVS,)), dma((2,)), dma((RECVS,)),
-        dma((2, 2)), dma((2, 3)), dma((2, 2)), dma((NZ,)), dma((2,)), dma((NZ,)), dma((22,)),
+        dma((2, 2)), dma((2, 4)), dma((2, 2)), dma((NZ,)), dma((2,)), dma((NZ,)), dma((22,)),
     ]
     return pl.pallas_call(
         kernel,

time: 71.8 us -> 71.1 us (level)
  no operation moved by 1% of the time
where the time goes in v5:
time: 71.1 us
  Pallas kernels  70.4 us (99%)
    pallas_call x1, Pallas kernels, local(): pl.pallas_call(kernel, out_shape=pltpu.VMEM((TOK, D), BF16), in_specs=spe...  70.4 us

profile of v5, /device:TPU:1, one launch (start us, length us, event | category | flops | bytes accessed | tf_op | source)
XLA Modules:
  0.0 71.1 jit_solution(3333213056507918245)
XLA Ops:
  0.0 70.4 %layer.1 = bf16[32,2048]{1,0:T(8,128)(2,1)S(1)} custom-call(bf16[256,128]{1,0:T(8,128)(2,1)} %mix_hbm.1, bf16[32,2048]{1,0:T(8,128)(2,1)} %stream_hbm.1, s32[1,256]{1,0:T(1,128)} %bitcast.19, f32[1,8]{1,0:T(1,128)} %bitcast.20, f32[8,64]{1,0:T(8,128)} %decay_hbm.1, f32[8,64]{1,0:T(8,128)} %freq_hbm.1, f32[256,64]{1,0:T(8,128)} %bitcast.13, ...), custom_call_target="tpu_custom_call" | custom-call | tf_op jit(solution)/shard_map/layer/pallas_call | solution.py:673
  70.4 0.7 copy.19

commit v6 on v5

--- a/solution.py
+++ b/solution.py
@@ -154,17 +154,18 @@
 RECVS = 34
 OFFSETS = (0, -1, 1, -2, 2, -3, 3, 4)
 ORDER = (
-    "maps", "gaz 1", "gby 1", "line", "gbz 1 0", "gay 0", "gay -1", "gaz 2", "share", "gay 1",
-    "gby 2", "gbz 1 1", "gbz 2 0", "scan", "out", "share2", "gay 2", "gaz 3", "gay -2", "gbz 1 2",
-    "dbz 1 0", "daz 1", "last", "gbz 2 1", "gay -3", "gbz 3 0", "gaz 4", "gay 3", "gbz 2 2",
-    "dby 1", "pass", "dbz 2 0", "day 0", "day -1", "proj", "day 1", "daz 2", "norm", "gbz 3 1",
-    "gay 4", "dby 2", "gbz 3 2", "dbz 1 1", "dbz 3 0", "day -2", "daz 3", "day 2", "dbz 1 2",
-    "gbz 4 0", "gbz 4 1", "gbz 4 2", "widen", "dal 1", "product 1", "dbz 2 1", "daz 4", "day -3",
-    "day 3", "dbz 2 2", "dal -2", "product -2", "dal -1", "product -1", "combine 1", "dal 2",
-    "product 2", "combine -2", "dal 0", "product 0", "combine -1", "combine 2", "dbz 3 1",
-    "combine 0", "day 4", "dbz 3 2", "dal -3", "product -3", "dal 3", "product 3", "combine -3",
-    "combine 3", "dbz 4 0", "dbz 4 1", "dbz 4 2", "dal 4", "product 4", "combine 4", "finish 1",
-    "finish -2", "finish -1", "finish 2", "finish 0", "finish -3", "finish 3", "finish 4",
+    "gby 1", "dby 1", "gaz 1", "line", "day 0", "gby 2", "daz 1", "gaz 2", "gbz 1 0", "gay 0",
+    "share", "gbz 1 2", "gay -1", "share2", "gay -2", "day -1", "maps", "gbz 1 1", "gaz 3",
+    "scan", "gbz 2 0", "gay 1", "out", "gay 2", "gbz 2 2", "gbz 2 1", "gay -3", "last", "gaz 4",
+    "daz 2", "gbz 3 0", "gbz 3 2", "dby 2", "gay 3", "pass", "gbz 3 1", "gay 4", "day 1", "day 2",
+    "daz 3", "dbz 1 1", "proj", "dbz 1 0", "dbz 1 2", "day -2", "norm", "gbz 4 0", "gbz 4 1",
+    "gbz 4 2", "widen", "daz 4", "dbz 2 1", "dal 1", "product 1", "dbz 2 0", "dal -1",
+    "product -1", "day -3", "day 3", "dbz 2 2", "combine 1", "dal 0", "product 0", "combine -1",
+    "dal 2", "product 2", "dal -2", "product -2", "dbz 3 1", "combine 0", "dbz 3 0", "day 4",
+    "dbz 3 2", "combine -2", "dal -3", "product -3", "dal 3", "product 3", "combine 2",
+    "combine -3", "dbz 4 0", "dbz 4 1", "dbz 4 2", "dal 4", "product 4", "combine 3", "combine 4",
+    "finish 1", "finish -1", "finish 0", "finish -2", "finish 2", "finish -3", "finish 3",
+    "finish 4",
 )
 
 

time: 71.1 us -> 69.7 us (0.980)
  Pallas kernels: 70.4 us -> 69 us
    pallas_call x1, Pallas kernels: 70.4 us -> 69 us  [local(): pl.pallas_call(kernel, out_shape=pltpu.VMEM((TOK, D), BF16), in_specs=spe...]
where the time goes in v6:
time: 69.7 us
  Pallas kernels  69 us (99%)
    pallas_call x1, Pallas kernels, local(): pl.pallas_call(kernel, out_shape=pltpu.VMEM((TOK, D), BF16), in_specs=spe...  69 us

profile of v6, /device:TPU:1, one launch (start us, length us, event | category | flops | bytes accessed | tf_op | source)
XLA Modules:
  0.0 69.7 jit_solution(17783598989067715067)
XLA Ops:
  0.0 69.0 %layer.1 = bf16[32,2048]{1,0:T(8,128)(2,1)S(1)} custom-call(bf16[256,128]{1,0:T(8,128)(2,1)} %mix_hbm.1, bf16[32,2048]{1,0:T(8,128)(2,1)} %stream_hbm.1, s32[1,256]{1,0:T(1,128)} %bitcast.19, f32[1,8]{1,0:T(1,128)} %bitcast.20, f32[8,64]{1,0:T(8,128)} %decay_hbm.1, f32[8,64]{1,0:T(8,128)} %freq_hbm.1, f32[256,64]{1,0:T(8,128)} %bitcast.13, ...), custom_call_target="tpu_custom_call" | custom-call | tf_op jit(solution)/shard_map/layer/pallas_call | solution.py:674
  69.0 0.7 copy.19

commit v7 on v6

--- a/solution.py
+++ b/solution.py
@@ -163,7 +163,7 @@
     "product -1", "day -3", "day 3", "dbz 2 2", "combine 1", "dal 0", "product 0", "combine -1",
     "dal 2", "product 2", "dal -2", "product -2", "dbz 3 1", "combine 0", "dbz 3 0", "day 4",
     "dbz 3 2", "combine -2", "dal -3", "product -3", "dal 3", "product 3", "combine 2",
-    "combine -3", "dbz 4 0", "dbz 4 1", "dbz 4 2", "dal 4", "product 4", "combine 3", "combine 4",
+    "combine -3", "dbz 4 0", "dbz 4 1", "dbz 4 2", "narrow 4", "dal 4", "product 4", "combine 3", "combine 4",
     "finish 1", "finish -1", "finish 0", "finish -2", "finish 2", "finish -3", "finish 3",
     "finish 4",
 )
@@ -552,16 +552,22 @@
         empty = jnp.zeros((T, FF - MAIN), BF16)
         hidden[:, MAIN:KPAD] = jnp.concatenate([tail, empty, empty, tail], axis=1)
 
-    def product(o):
-        zi = gu.zi(o)
-        at = pl.ds(zi * NY, NY)
-        out = dot_nt(hidden[:, 0:DA], dna[at].reshape(NY * ROWS, DA))
-        out = out + dot_nt(hidden[:, DA:MAIN], dnb[at, 0:ROWS].reshape(NY * ROWS, DB))
+    ready = {}
+
+    def narrow(o):
+        at = pl.ds(gu.zi(o) * NY, NY)
+        main = dot_nt(hidden[:, DA:MAIN], dnb[at, 0:ROWS].reshape(NY * ROWS, DB))
         rest = dnb[at, ROWS:DROWS].reshape(NY * ROWS // 2, DB)
-        sides = [dot_nt(hidden[:, at : at + 128], rest) for at in (MAIN, MAIN + 128)]
-        out = out + jnp.concatenate(
+        sides = [dot_nt(hidden[:, k : k + 128], rest) for k in (MAIN, MAIN + 128)]
+        ready[o] = main + jnp.concatenate(
             [side[:, k : k + ROWS // 2] for k in range(0, 128, ROWS // 2) for side in sides], axis=1
         )
+
+    def product(o):
+        if o not in ready:
+            narrow(o)
+        zi = gu.zi(o)
+        out = dot_nt(hidden[:, 0:DA], dna[pl.ds(zi * NY, NY)].reshape(NY * ROWS, DA)) + ready[o]
         out = out.astype(BF16).reshape(NX, NC, TOK, NY * ROWS)
         for k in range(NC):
             ffn_part[zi, k] = out[:, k]
@@ -595,7 +601,7 @@
         "maps": output_maps, "line": carry_line, "scan": scan, "out": mix_out, "share": share,
         "share2": share_rest, "last": share_last,
         "pass": mix_pass, "proj": project, "norm": normalize, "widen": widen,
-        "product": product, "combine": combine, "finish": finish,
+        "narrow": narrow, "product": product, "combine": combine, "finish": finish,
     }
     for step in ORDER:
         name, number = step.split()[0], [int(n) for n in step.split()[1:]]

time: 69.7 us -> 69.6 us (level)
  no operation moved by 1% of the time
where the time goes in v7:
time: 69.6 us; the launch traced here: 69.5 us
  Pallas kernels  68.9 us (99%)
    pallas_call x1, Pallas kernels, local(): pl.pallas_call(kernel, out_shape=pltpu.VMEM((TOK, D), BF16), in_specs=spe...  68.9 us

profile of v7, /device:TPU:1, one launch (start us, length us, event | category | flops | bytes accessed | tf_op | source)
XLA Modules:
  0.0 69.5 jit_solution(781443971052976398)
XLA Ops:
  0.0 68.9 %layer.1 = bf16[32,2048]{1,0:T(8,128)(2,1)S(1)} custom-call(bf16[256,128]{1,0:T(8,128)(2,1)} %mix_hbm.1, bf16[32,2048]{1,0:T(8,128)(2,1)} %stream_hbm.1, s32[1,256]{1,0:T(1,128)} %bitcast.19, f32[1,8]{1,0:T(1,128)} %bitcast.20, f32[8,64]{1,0:T(8,128)} %decay_hbm.1, f32[8,64]{1,0:T(8,128)} %freq_hbm.1, f32[256,64]{1,0:T(8,128)} %bitcast.13, ...), custom_call_target="tpu_custom_call" | custom-call | tf_op jit(solution)/shard_map/layer/pallas_call | solution.py:680
  68.9 0.7 copy.19
